TPU v7x, 32 devices: a whole 2x2x4 slice. The times are simulated.
32 devices in a mesh: ep: 8 (over z, x), tp: 4 (over y, core).
Axes of the slice: x: 2, y: 2, z: 4, core: 2. Of those that a mesh axis runs over, the one named last changes fastest.
Arguments:
- receptance: bfloat16 [2048, 1024], P('ep', 'tp'), may hold values from -6 to 6
- head_key_input: bfloat16 [2048, 1024], P('ep', 'tp'), may hold values from -12 to 12
- head_value_input: bfloat16 [2048, 1024], P('ep', 'tp'), may hold values from -6 to 6
- decay_input_part: bfloat16 [2048, 1024], P('ep', 'tp'), may hold values from -4 to 4
- learning_rate_input: bfloat16 [2048, 1024], P('ep', 'tp'), may hold values from -7 to 1
- output_gate_input: bfloat16 [2048, 1024], P('ep', 'tp'), may hold values from -6 to 6
- decay_channel_offset: float32 [1024], P('tp'), may hold values from -12.5 to -2
- spike_log_decay: float32 [2048, 1024], P('ep', 'tp'), may hold values from -0.7 to 0
- head_norm_gain: float32 [1024], P('tp'), may hold values from 0.1 to 1.9
- head_output_weight: bfloat16 [1024, 2048], P('tp'), may hold values from -0.25 to 0.25
- projection_norm_gain: float32 [2048], replicated, may hold values from 0.1 to 1.9
- expert_input_rows: bfloat16 [1024, 2048], P('ep'), may hold values from -6 to 6
- expert_norm_gain: float32 [2048], replicated, may hold values from 0.1 to 1.9
- selected_expert_index: int32 [1024, 2], P('ep'), may hold values from 0 to 15, all different within a row; in each aligned block of 128 rows (0 to 127, 128 to 255, ...) at most 32 rows name the same one
- selected_expert_weight: float32 [1024, 2], P('ep'), may hold values from 0.3 to 1.5
- routed_gate_weight: bfloat16 [32, 2048, 256], P(('ep', 'tp')), may hold values from -0.125 to 0.125
- routed_up_weight: bfloat16 [32, 2048, 256], P(('ep', 'tp')), may hold values from -0.125 to 0.125
- routed_down_weight: bfloat16 [32, 256, 2048], P(('ep', 'tp')), may hold values from -0.25 to 0.25
- common_gate_weight: bfloat16 [2048, 1024], P(None, 'tp'), may hold values from -0.125 to 0.125
- common_up_weight: bfloat16 [2048, 1024], P(None, 'tp'), may hold values from -0.125 to 0.125
- common_down_weight: bfloat16 [1024, 2048], P('tp'), may hold values from -0.25 to 0.25
Outputs:
- attention_output: bfloat16 [2048, 2048], P(('ep', 'tp'))
- expert_output: bfloat16 [1024, 2048], P('ep', 'tp')
Inputs may be any that keep to these rules, and one draw needn't show every extreme that they name: `selected_expert_index`: each row names 2 different experts. Among the rows of one index of ep (aligned blocks of 128 rows) no expert is named by more than 32 rows, a bound that some block reaches.
All inputs are finite; a program needn't handle non-finite values.
Results may differ from a plain program's by a relative error of at most 0.023.
Values may be sent and summed in bfloat16 or wider, within the bound.
A program may use at most 128 MiB of HBM per device.

v0:
```python
import functools

import jax
import jax.numpy as jnp
from jax import lax
from jax.experimental import pallas as pl
from jax.experimental.pallas import tpu as pltpu
from jax.sharding import PartitionSpec as P

HEAD_CHANNELS = 64
BLOCK = 64


MESH = pl.DeviceIdType.MESH
NORM_EPSILON = 1e-06
GROUP_EPSILON = 0.00064


def rms_scale(values, gain):
    values = values.astype(jnp.float32)
    return (
        values * lax.rsqrt(jnp.mean(values * values, axis=-1, keepdims=True) + NORM_EPSILON) * gain
    )


def split_parts(x):
    high = x.astype(jnp.bfloat16)
    return high, (x - high.astype(jnp.float32)).astype(jnp.bfloat16)


def dot3(x, y, dims):
    xh, xl = split_parts(x)
    yh, yl = split_parts(y)

    def one(p, q):
        return lax.dot_general(p, q, (dims, ((), ())), preferred_element_type=jnp.float32)

    return one(xh, yh) + (one(xh, yl) + one(xl, yh))


NN = ((1,), (0,))
NT = ((1,), (1,))
TN = ((0,), (0,))


def local_kernel(
    r_ref, k_ref, v_ref, dec_ref, lr_ref, off_ref, spike_ref, out_ref, carry_ref, map_ref
):
    rows, width = r_ref.shape
    heads = width // HEAD_CHANNELS
    blocks = rows // BLOCK
    row = lax.broadcasted_iota(jnp.int32, (rows, rows), 0)
    col = lax.broadcasted_iota(jnp.int32, (rows, rows), 1)
    strict = col < row
    inclusive = col <= row
    learn_all = jax.nn.sigmoid(lr_ref[...].astype(jnp.float32))
    pre = off_ref[...] + jnp.tanh(dec_ref[...].astype(jnp.float32))
    log_all = spike_ref[...] - jax.nn.sigmoid(pre) * jnp.exp(jnp.float32(-0.5))
    ones = jnp.where(inclusive, 1.0, 0.0).astype(jnp.bfloat16)
    p0 = log_all.astype(jnp.bfloat16)
    rest = log_all - p0.astype(jnp.float32)
    p1 = rest.astype(jnp.bfloat16)
    p2 = (rest - p1.astype(jnp.float32)).astype(jnp.bfloat16)
    cum_all = sum(jnp.dot(ones, p, preferred_element_type=jnp.float32) for p in (p0, p1, p2))
    before_all = cum_all - log_all
    for h in range(heads):
        lanes = slice(h * HEAD_CHANNELS, (h + 1) * HEAD_CHANNELS)
        r = r_ref[:, lanes].astype(jnp.float32)
        k = k_ref[:, lanes].astype(jnp.float32)
        v = v_ref[:, lanes].astype(jnp.float32)
        learn = learn_all[:, lanes]
        cum = cum_all[:, lanes]
        before = before_all[:, lanes]
        a = k * lax.rsqrt(jnp.sum(k * k, axis=-1, keepdims=True) + NORM_EPSILON)
        b = a * learn
        ins = k * learn
        parts = []
        for i in range(blocks):
            span = slice(i * BLOCK, (i + 1) * BLOCK)
            base = before[i * BLOCK : i * BLOCK + 1]
            left = jnp.concatenate(
                [a[span] * jnp.exp(before[span] - base), r[span] * jnp.exp(cum[span] - base)],
                axis=0,
            )
            back = jnp.exp(jnp.minimum(base - cum, 60.0))
            right = jnp.concatenate([b * back, ins * back], axis=0)
            parts.append(dot3(left, right, NT))
        low_b = jnp.where(strict, jnp.concatenate([p[:BLOCK, :rows] for p in parts], axis=0), 0.0)
        low_k = jnp.where(strict, jnp.concatenate([p[:BLOCK, rows:] for p in parts], axis=0), 0.0)
        out_b = jnp.where(
            inclusive, jnp.concatenate([p[BLOCK:, :rows] for p in parts], axis=0), 0.0
        )
        out_k = jnp.where(
            inclusive, jnp.concatenate([p[BLOCK:, rows:] for p in parts], axis=0), 0.0
        )
        inverse = jnp.where(row == col, 1.0, 0.0)
        size = 1
        while size < BLOCK:
            corner = (row // (2 * size) == col // (2 * size)) & (row // size != col // size)
            corner = jnp.where(corner, low_b, 0.0)
            if size == 1:
                inverse = inverse - corner
            else:
                inverse = inverse - dot3(dot3(inverse, corner, NN), inverse, NN)
            size *= 2
        right_side = jnp.concatenate([a * jnp.exp(before), dot3(low_k, v, NN)], axis=1)
        solved = []
        for i in range(blocks):
            span = slice(i * BLOCK, (i + 1) * BLOCK)
            piece = right_side[span]
            if i:
                piece = piece - dot3(
                    low_b[span, : i * BLOCK], jnp.concatenate(solved, axis=0), NN
                )
            solved.append(dot3(inverse[span, span], piece, NN))
        solved = jnp.concatenate(solved, axis=0)
        removed = dot3(out_b, solved, NN)
        out_ref[:, lanes] = dot3(out_k, v, NN) - removed[:, HEAD_CHANNELS:]
        carry_ref[:, lanes] = r * jnp.exp(cum) - removed[:, :HEAD_CHANNELS]
        last = cum[rows - 1 :]
        to_end = jnp.exp(last - cum)
        taken = dot3(solved, b * to_end, TN)
        added = dot3(v, ins * to_end, TN)
        small = (HEAD_CHANNELS, HEAD_CHANNELS)
        eye = lax.broadcasted_iota(jnp.int32, small, 0) == lax.broadcasted_iota(jnp.int32, small, 1)
        through = jnp.where(eye, jnp.exp(last), 0.0) - taken[:HEAD_CHANNELS]
        fresh = added - taken[HEAD_CHANNELS:]
        map_ref[lanes, :] = jnp.concatenate([through, fresh], axis=1).astype(jnp.bfloat16)


def join_kernel(
    count, out_ref, carry_ref, map_ref, gain_ref, gate_ref, weight_ref, mix_ref, held, state,
    send_sem, recv_sem
):
    me = lax.axis_index("ep")
    rows, width = out_ref.shape
    heads = width // HEAD_CHANNELS
    barrier = pltpu.get_barrier_semaphore()
    for step in range(1, count):
        pl.semaphore_signal(
            barrier, inc=1, device_id={"ep": lax.rem(me + step, count)}, device_id_type=MESH
        )
    pl.semaphore_wait(barrier, count - 1)

    def copy(slot, step):
        return pltpu.make_async_remote_copy(
            src_ref=map_ref,
            dst_ref=held.at[slot],
            send_sem=send_sem.at[step],
            recv_sem=recv_sem.at[slot],
            device_id={"ep": lax.rem(me + step, count)},
            device_id_type=MESH,
        )

    for step in range(1, count):

        @pl.when(me + step < count)
        def _():
            copy(me, step).start()

    state[...] = jnp.zeros_like(state)

    def one(turn, _):
        copy(turn, 1).wait_recv()
        for h in range(heads):
            lanes = slice(h * HEAD_CHANNELS, (h + 1) * HEAD_CHANNELS)
            block = held[turn, lanes, :]
            high, low = split_parts(state[lanes, :])
            through = block[:, :HEAD_CHANNELS]
            state[lanes, :] = (
                jnp.dot(high, through, preferred_element_type=jnp.float32)
                + jnp.dot(low, through, preferred_element_type=jnp.float32)
                + block[:, HEAD_CHANNELS:].astype(jnp.float32)
            )
        return 0

    lax.fori_loop(0, me, one, 0)
    normed = []
    for h in range(heads):
        lanes = slice(h * HEAD_CHANNELS, (h + 1) * HEAD_CHANNELS)
        value = out_ref[:, lanes] + dot3(carry_ref[:, lanes], state[lanes, :], NT)
        centred = value - jnp.mean(value, axis=-1, keepdims=True)
        normed.append(
            centred
            * lax.rsqrt(jnp.mean(centred * centred, axis=-1, keepdims=True) + GROUP_EPSILON)
        )
    flat = normed[0] if heads == 1 else jnp.concatenate(normed, axis=1)
    heads_out = flat * gain_ref[...] * jax.nn.sigmoid(gate_ref[...].astype(jnp.float32))
    mix_ref[...] = jnp.dot(
        heads_out.astype(jnp.bfloat16), weight_ref[...], preferred_element_type=jnp.float32
    ).astype(jnp.bfloat16)
    for step in range(1, count):

        @pl.when(me + step < count)
        def _():
            copy(me, step).wait_send()


def attention_mixer(
    receptance,
    head_key_input,
    head_value_input,
    decay_input_part,
    learning_rate_input,
    output_gate_input,
    decay_channel_offset,
    spike_log_decay,
    head_norm_gain,
    head_output_weight,
    projection_norm_gain,
):
    rows, width = receptance.shape
    count = lax.axis_size("ep")
    full = pl.BlockSpec(memory_space=pltpu.VMEM)
    out, carry, maps = pl.pallas_call(
        local_kernel,
        out_shape=(
            jax.ShapeDtypeStruct((rows, width), jnp.float32),
            jax.ShapeDtypeStruct((rows, width), jnp.float32),
            jax.ShapeDtypeStruct((width, 2 * HEAD_CHANNELS), jnp.bfloat16),
        ),
        in_specs=[full] * 7,
        out_specs=(full, full, full),
        cost_estimate=pl.CostEstimate(
            flops=rows * rows * width * 200, bytes_accessed=rows * width * 22, transcendentals=0
        ),
    )(
        receptance,
        head_key_input,
        head_value_input,
        decay_input_part,
        learning_rate_input,
        decay_channel_offset[None, :],
        spike_log_decay,
    )
    model_width = head_output_weight.shape[1]
    mix = pl.pallas_call(
        functools.partial(join_kernel, count),
        out_shape=jax.ShapeDtypeStruct((rows, model_width), jnp.bfloat16),
        in_specs=[full] * 6,
        out_specs=full,
        scratch_shapes=[
            pltpu.VMEM((count, width, 2 * HEAD_CHANNELS), jnp.bfloat16),
            pltpu.VMEM((width, HEAD_CHANNELS), jnp.float32),
            pltpu.SemaphoreType.DMA((count,)),
            pltpu.SemaphoreType.DMA((count,)),
        ],
        compiler_params=pltpu.CompilerParams(collective_id=0, has_side_effects=True),
        cost_estimate=pl.CostEstimate(
            flops=rows * width * model_width * 20,
            bytes_accessed=width * model_width * 2,
            transcendentals=0,
        ),
    )(out, carry, maps, head_norm_gain[None, :], output_gate_input, head_output_weight)
    mix_sum = lax.psum_scatter(mix, "tp", scatter_dimension=0, tiled=True).astype(jnp.float32)
    return rms_scale(mix_sum, projection_norm_gain).astype(jnp.bfloat16)


def expert_kernel(
    count, pairs, arrived, gate_ref, up_ref, down_ref, result_ref, crossing, halves, paired,
    final, back, half_send, half_recv, pair_send, pair_recv, back_send, back_recv
):
    me = lax.axis_index("ep")
    place = lax.axis_index("tp")
    group = place // 2
    half = place % 2
    capacity = arrived.shape[0] // count
    columns = final.shape[2]
    partner = 2 * group + 1 - half

    def rows_of(index):
        return pl.ds(pl.multiple_of(index * capacity, capacity), capacity)

    def peer(step):
        return lax.rem(me + step, count)

    barrier = pltpu.get_barrier_semaphore()
    for step in range(1, count):
        pl.semaphore_signal(barrier, inc=1, device_id={"ep": peer(step)}, device_id_type=MESH)
    pl.semaphore_signal(barrier, inc=1, device_id={"tp": partner}, device_id_type=MESH)
    for step in range(1, pairs):
        there = 2 * lax.rem(group + step, pairs) + half
        pl.semaphore_signal(barrier, inc=1, device_id={"tp": there}, device_id_type=MESH)
    pl.semaphore_wait(barrier, count + pairs - 1)

    def cross(index):
        return pltpu.make_async_remote_copy(
            src_ref=crossing.at[index],
            dst_ref=halves.at[index],
            send_sem=half_send.at[index],
            recv_sem=half_recv.at[index],
            device_id={"tp": partner},
            device_id_type=MESH,
        )

    def pair(step):
        return pltpu.make_async_remote_copy(
            src_ref=paired.at[step],
            dst_ref=final.at[step],
            send_sem=pair_send.at[step],
            recv_sem=pair_recv.at[step],
            device_id={"tp": 2 * lax.rem(group + step, pairs) + half},
            device_id_type=MESH,
        )

    def home(turn, step):
        return pltpu.make_async_remote_copy(
            src_ref=final.at[turn, rows_of(peer(step))],
            dst_ref=back.at[turn, rows_of(me)],
            send_sem=back_send.at[turn, step],
            recv_sem=back_recv.at[turn, step],
            device_id={"ep": peer(step)},
            device_id_type=MESH,
        )

    rows = arrived[...]
    gate = jnp.dot(rows, gate_ref[0], preferred_element_type=jnp.float32)
    upward = jnp.dot(rows, up_ref[0], preferred_element_type=jnp.float32)
    hidden = (jax.nn.silu(gate) * upward).astype(jnp.bfloat16)

    def part(index):
        span = pl.ds(pl.multiple_of(index * columns, columns), columns)
        return jnp.dot(hidden, down_ref[0, :, span], preferred_element_type=jnp.float32).astype(
            jnp.bfloat16
        )

    order = list(range(1, pairs)) + [0]
    for step in order:
        crossing[step] = part(2 * lax.rem(group + step, pairs) + 1 - half)
        cross(step).start()
    own = {step: part(2 * lax.rem(group + step, pairs) + half) for step in order}
    for step in order:
        cross(step).wait_recv()
        total = (
            own[step].astype(jnp.float32) + halves[step].astype(jnp.float32)
        ).astype(jnp.bfloat16)
        if step:
            paired[step] = total
            pair(step).start()
        else:
            final[0] = total
    for turn in range(pairs):
        if turn:
            pair(turn).wait_recv()
        for step in range(1, count):
            home(turn, step).start()
        back[turn, rows_of(me), :] = final[turn, rows_of(me), :]
    for turn in range(pairs):
        for step in range(1, count):
            home(turn, step).wait_recv()
        result_ref[lax.rem(group + pairs - turn, pairs)] = back[turn]
    for step in order:
        cross(step).wait_send()
        if step:
            pair(step).wait_send()
    for turn in range(pairs):
        for step in range(1, count):
            home(turn, step).wait_send()


def routed_by_kernel(arrived, gate_weight, up_weight, down_weight, count, pairs):
    rows, model_width = arrived.shape
    columns = model_width // (2 * pairs)
    full = pl.BlockSpec(memory_space=pltpu.VMEM)
    dma = pltpu.SemaphoreType.DMA
    block = pltpu.VMEM((pairs, rows, columns), jnp.bfloat16)
    return pl.pallas_call(
        functools.partial(expert_kernel, count, pairs),
        out_shape=jax.ShapeDtypeStruct((pairs, rows, columns), jnp.bfloat16),
        in_specs=[full] * 4,
        out_specs=full,
        scratch_shapes=[block] * 5
        + [dma((pairs,))] * 4
        + [dma((pairs, count))] * 2,
        compiler_params=pltpu.CompilerParams(collective_id=1, has_side_effects=True),
        cost_estimate=pl.CostEstimate(
            flops=10 * rows * model_width * gate_weight.shape[2] * 6,
            bytes_accessed=model_width * gate_weight.shape[2] * 6,
            transcendentals=0,
        ),
    )(arrived, gate_weight, up_weight, down_weight)


def routed_by_exchange(flat_rows, gate_weight, up_weight, down_weight, count, pairs):
    rows, model_width = flat_rows.shape
    columns = model_width // (2 * pairs)
    gate = jnp.dot(flat_rows, gate_weight[0], preferred_element_type=jnp.float32)
    upward = jnp.dot(flat_rows, up_weight[0], preferred_element_type=jnp.float32)
    hidden = (jax.nn.silu(gate) * upward).astype(jnp.bfloat16)
    partial_value = jnp.dot(hidden, down_weight[0], preferred_element_type=jnp.float32).astype(
        jnp.bfloat16
    )
    pieces = lax.all_to_all(partial_value[None], "tp", split_axis=2, concat_axis=0, tiled=True)
    paired = pieces.reshape(pairs, 2, rows, columns).astype(jnp.float32)
    expert_value = (
        (paired[:, 0] + paired[:, 1])
        .astype(jnp.bfloat16)
        .reshape(pairs, count, rows // count, columns)
    )
    returned = lax.all_to_all(expert_value, "ep", split_axis=1, concat_axis=1, tiled=True)
    return returned.reshape(-1, columns)


def expert_half(
    expert_input_rows,
    expert_norm_gain,
    selected_expert_index,
    selected_expert_weight,
    routed_gate_weight,
    routed_up_weight,
    routed_down_weight,
    common_gate_weight,
    common_up_weight,
    common_down_weight,
):
    tok_rows, model_width = expert_input_rows.shape
    chosen_count = selected_expert_index.shape[1]
    ep_count = lax.axis_size("ep")
    tp_count = lax.axis_size("tp")
    group_count = tp_count // 2
    expert_total = group_count * ep_count
    capacity = 2 * tok_rows * chosen_count // expert_total
    column_count = model_width // tp_count
    tp_place = lax.axis_index("tp")
    group_index = tp_place // 2
    normed = rms_scale(expert_input_rows, expert_norm_gain).astype(jnp.bfloat16)
    assigned = selected_expert_index.reshape(-1)
    assign_count = assigned.shape[0]
    expert_ids = jnp.arange(expert_total, dtype=jnp.int32)
    onehot = (assigned[:, None] == expert_ids[None, :]).astype(jnp.int32)
    ranking = jnp.sum((jnp.cumsum(onehot, axis=0) - onehot) * onehot, axis=1)
    target = jnp.where(
        assigned % group_count == group_index, assigned // group_count * capacity + ranking, -1
    ).reshape(tok_rows, chosen_count)
    slots = jnp.arange(ep_count * capacity, dtype=jnp.int32)
    placing = jnp.any(target[:, :, None] == slots[None, None, :], axis=1).astype(jnp.bfloat16)
    outgoing = lax.dot_general(
        placing, normed, (((0,), (0,)), ((), ())), preferred_element_type=jnp.float32
    ).astype(jnp.bfloat16)
    arrived = lax.all_to_all(
        outgoing.reshape(ep_count, capacity, model_width),
        "ep",
        split_axis=0,
        concat_axis=0,
        tiled=True,
    ).reshape(-1, model_width)
    if capacity % 16 == 0 and column_count % 128 == 0:
        flat_back = routed_by_kernel(
            arrived, routed_gate_weight, routed_up_weight, routed_down_weight, ep_count, group_count
        ).reshape(-1, column_count)
    else:
        flat_back = routed_by_exchange(
            arrived, routed_gate_weight, routed_up_weight, routed_down_weight, ep_count, group_count
        )
    position = (
        assigned % group_count * (ep_count * capacity)
        + assigned // group_count * capacity
        + ranking
    )
    picked = (
        jnp.take(flat_back, position, axis=0)
        .astype(jnp.float32)
        .reshape(tok_rows, chosen_count, column_count)
    )
    routed = jnp.sum(picked * selected_expert_weight[:, :, None], axis=1)
    shared_hidden = (
        jax.nn.silu(jnp.dot(normed, common_gate_weight, preferred_element_type=jnp.float32))
        * jnp.dot(normed, common_up_weight, preferred_element_type=jnp.float32)
    ).astype(jnp.bfloat16)
    shared_sum = lax.psum_scatter(
        lax.dot_general(
            common_down_weight,
            shared_hidden,
            (((0,), (1,)), ((), ())),
            preferred_element_type=jnp.float32,
        ).astype(jnp.bfloat16),
        "tp",
        scatter_dimension=0,
        tiled=True,
    ).astype(jnp.float32)
    return (routed + shared_sum.T).astype(jnp.bfloat16)


def body(
    receptance,
    head_key_input,
    head_value_input,
    decay_input_part,
    learning_rate_input,
    output_gate_input,
    decay_channel_offset,
    spike_log_decay,
    head_norm_gain,
    head_output_weight,
    projection_norm_gain,
    expert_input_rows,
    expert_norm_gain,
    selected_expert_index,
    selected_expert_weight,
    routed_gate_weight,
    routed_up_weight,
    routed_down_weight,
    common_gate_weight,
    common_up_weight,
    common_down_weight,
):
    attention_output = attention_mixer(
        receptance,
        head_key_input,
        head_value_input,
        decay_input_part,
        learning_rate_input,
        output_gate_input,
        decay_channel_offset,
        spike_log_decay,
        head_norm_gain,
        head_output_weight,
        projection_norm_gain,
    )
    expert_output = expert_half(
        expert_input_rows,
        expert_norm_gain,
        selected_expert_index,
        selected_expert_weight,
        routed_gate_weight,
        routed_up_weight,
        routed_down_weight,
        common_gate_weight,
        common_up_weight,
        common_down_weight,
    )
    return (attention_output, expert_output)


def solution(mesh):
    placed = (
        P("ep", "tp"),
        P("ep", "tp"),
        P("ep", "tp"),
        P("ep", "tp"),
        P("ep", "tp"),
        P("ep", "tp"),
        P("tp"),
        P("ep", "tp"),
        P("tp"),
        P("tp", None),
        P(),
        P("ep", None),
        P(),
        P("ep", None),
        P("ep", None),
        P(("ep", "tp"), None, None),
        P(("ep", "tp"), None, None),
        P(("ep", "tp"), None, None),
        P(None, "tp"),
        P(None, "tp"),
        P("tp", None),
    )
    return jax.shard_map(
        body,
        mesh=mesh,
        in_specs=placed,
        out_specs=(P(("ep", "tp"), None), P("ep", "tp")),
        check_vma=False,
    )
```

profile of v0, /device:TPU:0, one launch (start us, length us, event | category | flops | bytes accessed | tf_op | source)
XLA Modules:
  0.0 104.6 jit_solution(11222124128926658505)
XLA Ops:
  7.2 0.0 copy-start
  7.2 0.0 reduce-scatter.5.cloned.1.call-start
  7.2 1.3 %fusion.2 = f32[128]{0:T(128)S(1)} fusion(bf16[128,2048]{1,0:T(8,128)(2,1)} %param.32), kind=kLoop, calls=%fused_computation.8 | loop fusion | flops 786304 | bytes 524800 | tf_op jit(solution)/shard_map/reduce_sum | solution.py:22
  8.5 0.0 copy-start.1
  8.5 0.0 copy-start.3
  8.5 0.0 copy-start.7
  8.6 1.9 %fusion.28 = f32[128,256]{1,0:T(8,128)S(1)} fusion(bf16[2048,256]{1,0:T(8,128)(2,1)} %param.39, bf16[128,2048]{1,0:T(8,128)(2,1)} %param.32, f32[2048]{0:T(1024)} %param.33, f32[128]{0:T(128)S(1)} %add_rsqrt_fusion), kind=kOutput, calls=%fused_computation.62 | convolution fusion | flops 135266304 | bytes 1712640 | tf_op jit(solution)/shard_map/dot_general | solution.py:467
  10.4 0.0 copy-done
  10.5 0.0 copy-done.1
  10.5 0.0 copy-done.3
  10.5 0.0 copy-done.7
  10.5 0.0 copy-start.5
  10.5 1.6 %fusion = bf16[2048,128]{0,1:T(8,128)(2,1)} fusion(bf16[256,2048]{1,0:T(8,128)(2,1)S(1)} %copy-done, bf16[2048,256]{1,0:T(8,128)(2,1)S(1)} %copy-done.7, f32[128,256]{1,0:T(8,128)S(1)} %fusion.28, bf16[128,2048]{1,0:T(8,128)(2,1)S(1)} %copy-done.1, f32[2048]{0:T(1024)S(1)} %copy-done.3, f32[128]{0:T(128)S(1)} %add_rsqrt_fusion), kind=kOutput, calls=%fused_computation.3 | convolution fusion | flops 269942784 | bytes 3285504 | tf_op jit(solution)/shard_map/dot_general | solution.py:471
  12.1 0.0 reduce-scatter.5.cloned.1.call-update
  12.1 0.0 copy-done.5
  12.2 0.1 copy.39
  12.3 0.1 eq.50
  12.4 0.1 reshape.222
  12.6 0.6 reduce-window.6
  13.2 0.2 slice_reduce_fusion
  13.4 0.1 fusion.20
  13.5 0.1 reduce_sum.42
  13.6 0.1 copy.42
  13.8 0.1 add_select_fusion.2
  13.9 0.1 copy.48
  13.9 0.1 fusion.9
  14.1 1.6 %convolution_convert_fusion = bf16[256,2048]{1,0:T(8,128)(2,1)} fusion(pred[128,256]{1,0:T(8,128)(4,1)S(1)} %fusion.9, bf16[128,2048]{1,0:T(8,128)(2,1)S(1)} %copy-done.1, f32[2048]{0:T(1024)S(1)} %copy-done.3, f32[128]{0:T(128)S(1)} %add_rsqrt_fusion), kind=kOutput, calls=%fused_computation.1 | convolution fusion | flops 135790592 | bytes 1614336 | tf_op jit(solution)/shard_map/dot_general | solution.py:437
  15.6 7.3 %all-to-all-start = ((bf16[8,32,2048]{2,1,0:T(8,128)(2,1)}), bf16[8,32,2048]{2,1,0:T(8,128)(2,1)S(1)}, u32[]{:S(2)}, u32[]{:S(2)}) async-start(bf16[8,32,2048]{2,1,0:T(8,128)(2,1)} %bitcast.3), calls=%async_computation.1 | async-start | bytes 2097152 | tf_op jit(solution)/shard_map/all_to_all | solution.py:440
  22.9 0.2 reduce-scatter.3.cloned.1.call-start
  23.1 21.6 %shard_map.212 = (f32[256,256]{1,0:T(8,128)}, f32[256,256]{1,0:T(8,128)}, bf16[256,128]{1,0:T(8,128)(2,1)}) custom-call(bf16[256,256]{1,0:T(8,128)(2,1)} %r_ref.1, bf16[256,256]{1,0:T(8,128)(2,1)} %k_ref.1, bf16[256,256]{1,0:T(8,128)(2,1)} %v_ref.1, bf16[256,256]{1,0:T(8,128)(2,1)} %dec_ref.1, bf16[256,256]{1,0:T(8,128)(2,1)} %lr_ref.1, f32[1,256]{1,0:T(1,128)} %bitcast.40, ...), custom_call_target="tpu_custom_call" | custom-call | flops 3355443200 | bytes 1441792 | tf_op jit(solution)/shard_map/pallas_call | solution.py:215
  44.7 14.9 %shard_map.213 = bf16[256,2048]{1,0:T(8,128)(2,1)} custom-call(f32[256,256]{1,0:T(8,128)} %get-tuple-element.5.out_ref, f32[256,256]{1,0:T(8,128)} %get-tuple-element.6.carry_ref, bf16[256,128]{1,0:T(8,128)(2,1)} %get-tuple-element.7.map_ref, f32[1,256]{1,0:T(1,128)} %bitcast.41, bf16[256,256]{1,0:T(8,128)(2,1)} %gate_ref.2, bf16[256,2048]{1,0:T(8,128)(2,1)} %weight_ref.1), custom_call_target="tpu_custom_call" | custom-call | flops 2684354560 | bytes 1048576 | tf_op jit(solution)/shard_map/pallas_call | solution.py:237
  59.6 0.0 copy-start.6
  59.7 0.0 reduce-scatter.3.cloned.1.call-update
  59.7 0.1 reshape.227
  59.8 0.5 copy-done.6
  60.3 0.1 copy.50
  60.5 0.1 compare_and_fusion
  60.6 0.0 all-to-all-done
  60.6 0.0 copy-start.2
  60.6 1.0 copy-done.2
  61.6 28.3 %shard_map.214 = bf16[2,256,512]{2,1,0:T(8,128)(2,1)} custom-call(bf16[256,2048]{1,0:T(8,128)(2,1)} %bitcast.37, bf16[1,2048,256]{2,1,0:T(8,128)(2,1)} %gate_ref.3, bf16[1,2048,256]{2,1,0:T(8,128)(2,1)} %up_ref.1, bf16[1,256,2048]{2,1,0:T(8,128)(2,1)} %down_ref.1), custom_call_target="tpu_custom_call" | custom-call | flops 8053063680 | bytes 3145728 | tf_op jit(solution)/shard_map/pallas_call | solution.py:367
  89.9 2.3 %gather_fusion = bf16[256,512]{1,0:T(8,128)(2,1)S(1)} fusion(bf16[512,512]{1,0:T(8,128)(2,1)} %bitcast.36, s32[1024]{0:T(1024)S(1)} %pad_clamp_fusion), kind=kCustom, calls=%fused_computation | custom fusion | bytes 525312 | tf_op jit(solution)/shard_map/jit(_take)/gather | solution.py:461
  92.2 0.0 copy-start.4
  92.2 0.1 gather.7
  92.3 0.8 multiply_reduce_fusion
  93.2 0.0 reduce-scatter.5.cloned.1.call-done
  93.2 1.6 %fusion.8 = bf16[128,512]{1,0:T(8,128)(2,1)} fusion(f32[128,512]{1,0:T(8,128)S(1)} %multiply_reduce_fusion, bf16[512,128]{0,1:T(8,128)(2,1)} %reduce-scatter.5.cloned.1.call-done), kind=kLoop, calls=%fused_computation.19 | loop fusion | flops 196608 | bytes 524288 | tf_op jit(solution)/shard_map/convert_element_type | solution.py:481
  94.8 0.0 reduce-scatter.3.cloned.1.call-done
  94.8 1.1 %fusion.5 = f32[64]{0:T(128)S(1)} fusion(bf16[64,2048]{1,0:T(8,128)(2,1)} %reduce-scatter.3.cloned.1.call-done), kind=kLoop, calls=%fused_computation.13 | loop fusion | flops 393152 | bytes 262400 | tf_op jit(solution)/shard_map/reduce_sum | solution.py:22
  95.9 0.0 copy-done.4
  95.9 1.8 %fusion.7 = bf16[64,2048]{1,0:T(8,128)(2,1)} fusion(bf16[64,2048]{1,0:T(8,128)(2,1)} %reduce-scatter.3.cloned.1.call-done, f32[2048]{0:T(1024)S(1)} %copy-done.4, f32[64]{0:T(128)S(1)} %add_rsqrt_fusion.1), kind=kLoop, calls=%fused_computation.15 | loop fusion | flops 524288 | bytes 532736 | tf_op jit(solution)/shard_map/convert_element_type | solution.py:256
  (8 shorter events, 0.1 us)
Async XLA Ops:
  7.2 3.3 %copy-start = (bf16[256,2048]{1,0:T(8,128)(2,1)S(1)}, bf16[256,2048]{1,0:T(8,128)(2,1)}, u32[]{:S(2)}) copy-start(bf16[256,2048]{1,0:T(8,128)(2,1)} %param.41) | copy-start | bytes 3145732
  7.2 86.0 %reduce-scatter.5.cloned.1.call-start = ((), (), s32[]{:S(2)}) async-start(), calls=%async_computation.4 | async-start | bytes 655360 | tf_op jit(solution)/shard_map/reduce_scatter | solution.py:470
  8.5 1.9 %copy-start.1 = (bf16[128,2048]{1,0:T(8,128)(2,1)S(1)}, bf16[128,2048]{1,0:T(8,128)(2,1)}, u32[]{:S(2)}) copy-start(bf16[128,2048]{1,0:T(8,128)(2,1)} %param.32) | copy-start | bytes 1572868
  8.5 1.9 %copy-start.3 = (f32[2048]{0:T(1024)S(1)}, f32[2048]{0:T(1024)}, u32[]{:S(2)}) copy-start(f32[2048]{0:T(1024)} %param.33) | copy-start | bytes 24580
  8.5 1.9 %copy-start.7 = (bf16[2048,256]{1,0:T(8,128)(2,1)S(1)}, bf16[2048,256]{1,0:T(8,128)(2,1)}, u32[]{:S(2)}) copy-start(bf16[2048,256]{1,0:T(8,128)(2,1)} %param.40) | copy-start | bytes 3145732
  10.5 1.7 %copy-start.5 = (s32[128,2]{0,1:T(2,128)S(1)}, s32[128,2]{0,1:T(2,128)}, u32[]{:S(2)}) copy-start(s32[128,2]{0,1:T(2,128)} %param.34) | copy-start | bytes 3076
  15.6 44.9 %all-to-all-start = ((bf16[8,32,2048]{2,1,0:T(8,128)(2,1)}), bf16[8,32,2048]{2,1,0:T(8,128)(2,1)S(1)}, u32[]{:S(2)}, u32[]{:S(2)}) async-start(bf16[8,32,2048]{2,1,0:T(8,128)(2,1)} %bitcast.3), calls=%async_computation.1 | async-start | bytes 2097152 | tf_op jit(solution)/shard_map/all_to_all | solution.py:440
  22.9 71.9 %reduce-scatter.3.cloned.1.call-start = ((), (), s32[]{:S(2)}) async-start(), calls=%async_computation.3 | async-start | bytes 1310720 | tf_op jit(solution)/shard_map/reduce_scatter | solution.py:255
  59.6 0.7 copy-start.6
  60.6 1.0 copy-start.2
  92.2 3.7 %copy-start.4 = (f32[2048]{0:T(1024)S(1)}, f32[2048]{0:T(1024)}, u32[]{:S(2)}) copy-start(f32[2048]{0:T(1024)} %param.31) | copy-start | bytes 24580
Sparse Core Ops, SparseCore 0:
  12.3 24.3 reduce-scatter.4
  59.8 31.1 reduce-scatter.2
where the time goes:
time: 105 us
  Pallas kernels  64.8 us (62%)
  between operations  14.3 us (14%)
  other arithmetic  7.68 us (7%)
  starting transfers between devices  7.54 us (7%)
  local copies, waits for them, and re-layouts  5.17 us (5%)
  matrix products  5.05 us (5%)
    pallas_call x1, Pallas kernels, routed_by_kernel(): pl.pallas_call(functools.partial(expert_kernel, count, pairs), out_shape=...  28.3 us
    pallas_call x1, Pallas kernels, attention_mixer(): pl.pallas_call(local_kernel, out_shape=(jax.ShapeDtypeStruct((rows, width...  21.6 us
    pallas_call x1, Pallas kernels, attention_mixer(): pl.pallas_call(functools.partial(join_kernel, count), out_shape=jax.Shape...  14.9 us
    all_to_all x1, starting transfers between devices, expert_half(): lax.all_to_all(outgoing.reshape(ep_count, capacity, model_width), 'ep', s...  7.28 us
    gather x2, local copies, waits for them, and re-layouts, expert_half(): jnp.take(flat_back, position, axis=0).astype(jnp.float32)  2.42 us
    reduce_sum x2, other arithmetic, rms_scale(): jnp.mean(values * values, axis=-1, keepdims=True) + NORM_EPSILON  2.41 us
  transfers between devices with their start and end apart: 3, of which 0 were waited for; matrix products, arithmetic and copies ran while one was open for 8% of the time, Pallas kernels for 62%

commit v1 on v0

--- a/solution.py
+++ b/solution.py
@@ -481,6 +481,673 @@
     return (routed + shared_sum.T).astype(jnp.bfloat16)
 
 
+def mm(x, y, dims=NN):
+    return lax.dot_general(x, y, (dims, ((), ())), preferred_element_type=jnp.float32)
+
+
+def pair_masks():
+    lane = lax.broadcasted_iota(jnp.int32, (BLOCK, 2 * HEAD_CHANNELS), 1)
+    first = jnp.where(lane < HEAD_CHANNELS, 1.0, 0.0)
+    return first.astype(jnp.bfloat16), (1.0 - first).astype(jnp.bfloat16)
+
+
+def stacked(y, masks):
+    return jnp.concatenate([y * masks[0], y * masks[1]], axis=0)
+
+
+def pair_dot(x, parts):
+    xh, xl = split_parts(x)
+    high, low = parts
+    return mm(jnp.concatenate([xh, xl], axis=1), jnp.concatenate([high, high], axis=0)) + mm(
+        xh, low
+    )
+
+
+def pair_parts(y, masks):
+    yh, yl = split_parts(y)
+    return stacked(yh, masks), stacked(yl, masks)
+
+
+def side_by_side(one, two):
+    return tuple(jnp.concatenate([p, q], axis=1) for p, q in zip(one, two))
+
+
+def head_sum(x, block_ones):
+    xh, xl = split_parts(x)
+    return mm(jnp.concatenate([xh, xl], axis=1), block_ones)
+
+
+def head_ones():
+    wide = 2 * HEAD_CHANNELS
+    row = lax.broadcasted_iota(jnp.int32, (2 * wide, wide), 0)
+    col = lax.broadcasted_iota(jnp.int32, (2 * wide, wide), 1)
+    same = (row // HEAD_CHANNELS) % 2 == col // HEAD_CHANNELS
+    return jnp.where(same, 1.0, 0.0).astype(jnp.bfloat16)
+
+
+def local_math(r_ref, k_ref, v_ref, dec_ref, lr_ref, off_ref, spike_ref):
+    rows, width = r_ref.shape
+    wide = 2 * HEAD_CHANNELS
+    pairs = width // wide
+    chunks = rows // BLOCK
+    masks = pair_masks()
+    ones_head = head_ones()
+    row = lax.broadcasted_iota(jnp.int32, (BLOCK, wide), 0)
+    col = lax.broadcasted_iota(jnp.int32, (BLOCK, wide), 1) % HEAD_CHANNELS
+    strict = col < row
+    inclusive = col <= row
+    trow = lax.broadcasted_iota(jnp.int32, (BLOCK, 4 * BLOCK), 0)
+    tcol = lax.broadcasted_iota(jnp.int32, (BLOCK, 4 * BLOCK), 1)
+    running = jnp.where((tcol % BLOCK <= trow) & (tcol < 3 * BLOCK), 1.0, 0.0).astype(jnp.bfloat16)
+    blank = jnp.zeros((BLOCK, wide), jnp.bfloat16)
+    items = [(i, p) for i in range(chunks) for p in range(pairs)]
+    lows, low_vs, out_bs, out_vs, ins_ends, b_ends, r_outs, a_ins, vs, ends = (
+        [] for _ in range(10)
+    )
+    for i, p in items:
+        span = slice(i * BLOCK, (i + 1) * BLOCK)
+        lanes = slice(p * wide, (p + 1) * wide)
+        r = r_ref[span, lanes].astype(jnp.float32)
+        k = k_ref[span, lanes].astype(jnp.float32)
+        v = v_ref[span, lanes]
+        learn = jax.nn.sigmoid(lr_ref[span, lanes].astype(jnp.float32))
+        pre = off_ref[:, lanes] + jnp.tanh(dec_ref[span, lanes].astype(jnp.float32))
+        log = spike_ref[span, lanes] - jax.nn.sigmoid(pre) * jnp.exp(jnp.float32(-0.5))
+        p0 = log.astype(jnp.bfloat16)
+        rest = log - p0.astype(jnp.float32)
+        p1 = rest.astype(jnp.bfloat16)
+        p2 = (rest - p1.astype(jnp.float32)).astype(jnp.bfloat16)
+        cum = mm(running, jnp.concatenate([p0, p1, p2, blank], axis=0))
+        before = cum - log
+        last = cum[BLOCK - 1 :]
+        a = k * lax.rsqrt(head_sum(k * k, ones_head) + NORM_EPSILON)
+        back = jnp.exp(-cum)
+        end = jnp.exp(last)
+        a_in = a * jnp.exp(before)
+        r_out = r * jnp.exp(cum)
+        b_back = a * learn * back
+        ins_back = k * learn * back
+        lh, ll = split_parts(jnp.concatenate([a_in, r_out], axis=0))
+        bh, bl = split_parts(b_back)
+        ih, il = split_parts(ins_back)
+        right_high = jnp.concatenate([stacked(bh, masks), stacked(ih, masks)], axis=0)
+        right_low = jnp.concatenate([stacked(bl, masks), stacked(il, masks)], axis=0)
+        gram = mm(
+            jnp.concatenate([lh, ll], axis=1),
+            jnp.concatenate([right_high, right_high], axis=1),
+            NT,
+        ) + mm(lh, right_low, NT)
+        lows.append(jnp.where(strict, gram[:BLOCK, :wide], 0.0))
+        low_k = jnp.where(strict, gram[:BLOCK, wide:], 0.0)
+        out_bs.append(jnp.where(inclusive, gram[BLOCK:, :wide], 0.0))
+        out_k = jnp.where(inclusive, gram[BLOCK:, wide:], 0.0)
+        kh, kl = split_parts(jnp.concatenate([low_k, out_k], axis=0))
+        values = stacked(v, masks)
+        weighted = mm(
+            jnp.concatenate([kh, kl], axis=1), jnp.concatenate([values, values], axis=0)
+        )
+        low_vs.append(weighted[:BLOCK])
+        out_vs.append(weighted[BLOCK:])
+        ins_ends.append(ins_back * end)
+        b_ends.append(b_back * end)
+        r_outs.append(r_out)
+        a_ins.append(a_in)
+        vs.append(v)
+        ends.append(end)
+    count = range(len(items))
+    eye = jnp.where(row == col, 1.0, 0.0)
+    inverses = None
+    size = 1
+    while size < BLOCK:
+        inside = (row // (2 * size) == col // (2 * size)) & (row // size != col // size)
+        corners = [jnp.where(inside, low, 0.0) for low in lows]
+        if size == 1:
+            inverses = [eye - corner for corner in corners]
+        else:
+            firsts = [
+                pair_dot(inverses[n], pair_parts(corners[n], masks)) for n in count
+            ]
+            inverses = [
+                inverses[n] - pair_dot(firsts[n], pair_parts(inverses[n], masks)) for n in count
+            ]
+        size *= 2
+    solved = [
+        side_by_side(pair_parts(a_ins[n], masks), pair_parts(low_vs[n], masks)) for n in count
+    ]
+    solved = [pair_dot(inverses[n], solved[n]) for n in count]
+    brow = lax.broadcasted_iota(jnp.int32, (wide, 2 * wide), 0)
+    bcol = lax.broadcasted_iota(jnp.int32, (wide, 2 * wide), 1)
+    same_head = brow // HEAD_CHANNELS == (bcol % wide) // HEAD_CHANNELS
+    diagonal = brow == bcol
+    maps = []
+    for n in count:
+        left = jnp.concatenate([-b_ends[n], ins_ends[n]], axis=0)
+        lh, ll = split_parts(left)
+        uh, ul = split_parts(solved[n])
+        high = jnp.concatenate([uh, jnp.concatenate([blank, vs[n]], axis=1)], axis=0)
+        low = jnp.concatenate([ul, jnp.concatenate([blank, blank], axis=1)], axis=0)
+        made = mm(
+            jnp.concatenate([lh, ll], axis=0), jnp.concatenate([high, high], axis=0), TN
+        ) + mm(lh, low, TN)
+        end = jnp.concatenate([ends[n], ends[n]], axis=1)
+        maps.append(jnp.where(same_head, made + jnp.where(diagonal, end, 0.0), 0.0))
+    whole = [None] * pairs
+    heads_at = []
+    for n in count:
+        p = items[n][1]
+        heads_at.append(whole[p])
+        if whole[p] is None:
+            whole[p] = maps[n]
+        else:
+            joined = pair_dot(maps[n][:, :wide], split_parts(whole[p]))
+            whole[p] = jnp.concatenate(
+                [joined[:, :wide], joined[:, wide:] + maps[n][:, wide:]], axis=1
+            )
+    compact = [m[:HEAD_CHANNELS] + m[HEAD_CHANNELS:] for m in whole]
+
+    def finish():
+        results = {}
+        for n in count:
+            uh, ul = split_parts(solved[n])
+            parts = [
+                jnp.concatenate([stacked(u[:, :wide], masks), stacked(u[:, wide:], masks)], axis=1)
+                for u in (uh, ul)
+            ]
+            removed = pair_dot(out_bs[n], parts)
+            carry = r_outs[n] - removed[:, :wide]
+            value = out_vs[n] - removed[:, wide:]
+            if heads_at[n] is not None:
+                moved = pair_dot(carry, split_parts(heads_at[n]))
+                carry = moved[:, :wide]
+                value = value + moved[:, wide:]
+            results[items[n]] = (carry, value)
+        return results
+
+    return compact, finish
+
+
+def mega_kernel(ep_count, *refs):
+    (
+        r_in, k_in, v_in, dec_in, lr_in, gate_in, off_in, spike_in, hgain_in, wout_in, pgain_in,
+        x_in, egain_in, idx_in, wsel_in, wg_in, wu_in, wd_in, cg_in, cu_in, cd_in,
+    ) = refs[:21]
+    attn_out, expert_out = refs[21:23]
+    (
+        r_ref, k_ref, v_ref, dec_ref, lr_ref, gate_ref, off_ref, spike_ref, hgain_ref, wout_ref,
+        pgain_ref, x_ref, egain_ref, idx_ref, wsel_ref, wg_ref, wu_ref, wd_ref, cg_ref, cu_ref,
+        cd_ref,
+    ) = refs[23:44]
+    (
+        normed, outgoing, arrived, carry_ref, value_ref, own_map, part_map, own_join, held, state,
+        shared, shared_half, shared_sum, shared_last, crossing, halves, own_ref, final, back,
+        heads_ref, mix, mix_half, mix_sum, mix_last,
+        load_sem, disp_send, disp_recv, fwd_send, fwd_recv, map_send, map_recv, join_send,
+        join_recv, sh_send, sh_recv, cross_send, cross_recv, home_send, home_recv, mx_send,
+        mx_recv, tail_send, tail_recv,
+    ) = refs[44:]
+    me = lax.axis_index("ep")
+    place = lax.axis_index("tp")
+    group = place // 2
+    half = place % 2
+    other = 1 - half
+    partner = 2 * group + other
+    across = 2 * (1 - group) + half
+    seat = me // 2
+    side = me % 2
+    seats = ep_count // 2
+    tok_rows, model_width = x_ref.shape
+    slots = outgoing.shape[0]
+    capacity = slots // ep_count
+    fold = model_width // 2
+    columns = model_width // 4
+    rows, width = r_ref.shape
+    wide = 2 * HEAD_CHANNELS
+    pairs = width // wide
+    block_rows = rows // 4
+
+    barrier = pltpu.get_barrier_semaphore()
+
+    def peer(step):
+        return lax.rem(me + step, ep_count)
+
+    for step in range(ep_count):
+        for turn in range(2):
+            if step or turn:
+                pl.semaphore_signal(
+                    barrier,
+                    inc=1,
+                    device_id={
+                        "ep": peer(step),
+                        "tp": 2 * lax.rem(group + turn, 2) + half,
+                    },
+                    device_id_type=MESH,
+                )
+    pl.semaphore_signal(barrier, inc=1, device_id={"tp": partner}, device_id_type=MESH)
+
+    sources = (
+        r_in, k_in, v_in, dec_in, lr_in, gate_in, off_in, spike_in, hgain_in, wout_in, pgain_in,
+        x_in, egain_in, idx_in, wsel_in, wg_in, wu_in, wd_in, cg_in, cu_in, cd_in,
+    )
+    targets = (
+        r_ref, k_ref, v_ref, dec_ref, lr_ref, gate_ref, off_ref, spike_ref, hgain_ref, wout_ref,
+        pgain_ref, x_ref, egain_ref, idx_ref, wsel_ref, wg_ref, wu_ref, wd_ref, cg_ref, cu_ref,
+        cd_ref,
+    )
+    loads = [
+        pltpu.make_async_copy(source, target, load_sem.at[n])
+        for n, (source, target) in enumerate(zip(sources, targets))
+    ]
+    for n in (11, 12, 13, 14, 0, 1, 2, 3, 4, 6, 7, 18, 19, 20, 15, 16, 17, 5, 8, 9, 10):
+        loads[n].start()
+
+    def rows_of(index):
+        return pl.ds(pl.multiple_of(index * capacity, capacity), capacity)
+
+    def remote(source, target, send, recv, where):
+        return pltpu.make_async_remote_copy(
+            src_ref=source,
+            dst_ref=target,
+            send_sem=send,
+            recv_sem=recv,
+            device_id=where,
+            device_id_type=MESH,
+        )
+
+    def dispatch(step):
+        return remote(
+            outgoing.at[rows_of(peer(step))],
+            arrived.at[half, rows_of(me)],
+            disp_send.at[step],
+            disp_recv.at[step],
+            {"ep": peer(step)},
+        )
+
+    def forward(step):
+        came = lax.rem(me + ep_count - step, ep_count)
+        return remote(
+            arrived.at[half, rows_of(came)],
+            arrived.at[half, rows_of(came)],
+            fwd_send.at[step],
+            fwd_recv.at[step],
+            {"tp": partner},
+        )
+
+    for n in (11, 12, 13, 14):
+        loads[n].wait()
+    normed[...] = rms_scale(x_ref[...], egain_ref[...]).astype(jnp.bfloat16)
+    chosen_count = idx_ref.shape[0]
+    experts = 2 * ep_count
+    expert_row = lax.broadcasted_iota(jnp.int32, (experts, tok_rows), 0)
+    named = [expert_row == idx_ref[k : k + 1, :] for k in range(chosen_count)]
+    member = functools.reduce(jnp.logical_or, named)
+    weight_of = functools.reduce(
+        jnp.add, [jnp.where(n, wsel_ref[k : k + 1, :], 0.0) for k, n in enumerate(named)]
+    )
+    early = lax.broadcasted_iota(jnp.int32, (tok_rows, tok_rows), 0) < lax.broadcasted_iota(
+        jnp.int32, (tok_rows, tok_rows), 1
+    )
+    rank = mm(
+        jnp.where(member, 1.0, 0.0).astype(jnp.bfloat16),
+        jnp.where(early, 1.0, 0.0).astype(jnp.bfloat16),
+    )
+    rank = jnp.where(member, rank, -1.0).astype(jnp.bfloat16)
+    slot = lax.broadcasted_iota(jnp.int32, (slots, experts), 0)
+    which = lax.broadcasted_iota(jnp.int32, (slots, experts), 1)
+    mine = jnp.where(which == 2 * (slot // capacity) + group, 1.0, 0.0).astype(jnp.bfloat16)
+    slot_rank = (
+        lax.broadcasted_iota(jnp.int32, (slots, tok_rows), 0) % capacity
+    ).astype(jnp.float32)
+    placing = jnp.where(mm(mine, rank) == slot_rank, 1.0, 0.0).astype(jnp.bfloat16)
+    fold_span = pl.ds(pl.multiple_of(half * fold, fold), fold)
+    outgoing[...] = mm(placing, normed[:, fold_span]).astype(jnp.bfloat16)
+    arrived[half, rows_of(me), :] = outgoing[rows_of(me), :]
+    pl.semaphore_wait(barrier, 2 * ep_count)
+    order = list(range(1, ep_count))
+    for step in order:
+        dispatch(step).start()
+    forward(0).start()
+
+    for n in (0, 1, 2, 3, 4, 6, 7):
+        loads[n].wait()
+    compact, finish = local_math(r_ref, k_ref, v_ref, dec_ref, lr_ref, off_ref, spike_ref)
+    for p in range(pairs):
+        own_map[p] = compact[p].astype(jnp.bfloat16)
+    swap = remote(
+        own_map, part_map, map_send.at[0], map_recv.at[0], {"ep": 2 * seat + 1 - side}
+    )
+    swap.start()
+    for (i, p), (carry, value) in finish().items():
+        span = slice(i * BLOCK, (i + 1) * BLOCK)
+        lanes = slice(p * wide, (p + 1) * wide)
+        carry_ref[span, lanes] = carry
+        value_ref[span, lanes] = value
+
+    masks = pair_masks()
+    swap.wait_recv()
+    for p in range(pairs):
+        mine_map = own_map[p]
+        their_map = part_map[p]
+        first = jnp.where(side == 0, mine_map, their_map)
+        second = jnp.where(side == 0, their_map, mine_map)
+        blocks = jnp.concatenate(
+            [stacked(first[:, :wide], masks), stacked(first[:, wide:], masks)], axis=1
+        )
+        joined = mm(second[:, :wide], blocks)
+        own_join[p] = jnp.concatenate(
+            [joined[:, :wide], joined[:, wide:] + second[:, wide:].astype(jnp.float32)], axis=1
+        ).astype(jnp.bfloat16)
+
+    def upward(step):
+        return remote(
+            own_join,
+            held.at[seat],
+            join_send.at[step],
+            join_recv.at[seat],
+            {"ep": lax.rem(me + 2 * step, ep_count)},
+        )
+
+    def arrival(turn):
+        return remote(
+            own_join, held.at[turn], join_send.at[1], join_recv.at[turn],
+            {"ep": lax.rem(me + 2, ep_count)},
+        )
+
+    for step in range(1, seats):
+
+        @pl.when(seat + step < seats)
+        def _():
+            upward(step).start()
+
+    for n in (18, 19, 20):
+        loads[n].wait()
+    rows_in = normed[...]
+    hidden = (jax.nn.silu(mm(rows_in, cg_ref[...])) * mm(rows_in, cu_ref[...])).astype(
+        jnp.bfloat16
+    )
+    for j in range(4):
+        shared[j] = mm(hidden, cd_ref[:, j * columns : (j + 1) * columns]).astype(jnp.bfloat16)
+
+    def shared_cross(g):
+        return remote(
+            shared.at[2 * g + other],
+            shared_half.at[g],
+            sh_send.at[g],
+            sh_recv.at[g],
+            {"tp": partner},
+        )
+
+    for g in range(2):
+        shared_cross(g).start()
+
+    for n in (15, 16, 17):
+        loads[n].wait()
+    for step in order:
+        dispatch(step).wait_recv()
+        forward(step).start()
+    other_span = pl.ds(pl.multiple_of(other * fold, fold), fold)
+    own_rows = arrived[half]
+    gate = mm(own_rows, wg_ref[fold_span, :])
+    upper = mm(own_rows, wu_ref[fold_span, :])
+
+    for g in range(2):
+        shared_cross(g).wait_recv()
+        shared_sum[g] = shared[2 * g + half].astype(jnp.float32) + shared_half[g].astype(
+            jnp.float32
+        )
+    shared_last[0] = shared_sum[1 - group].astype(jnp.bfloat16)
+    shared_tail = remote(
+        shared_last.at[0], shared_last.at[1], tail_send.at[0], tail_recv.at[0], {"tp": across}
+    )
+    shared_tail.start()
+
+    for step in range(ep_count):
+        forward(step).wait_recv()
+    other_rows = arrived[other]
+    gate = gate + mm(other_rows, wg_ref[other_span, :])
+    upper = upper + mm(other_rows, wu_ref[other_span, :])
+    routed_hidden = (jax.nn.silu(gate) * upper).astype(jnp.bfloat16)
+
+    def part(index):
+        span = pl.ds(pl.multiple_of(index * columns, columns), columns)
+        return mm(routed_hidden, wd_ref[:, span])
+
+    def cross(turn):
+        return remote(
+            crossing.at[turn],
+            halves.at[turn],
+            cross_send.at[turn],
+            cross_recv.at[turn],
+            {"tp": partner},
+        )
+
+    turn_order = (1, 0)
+    for turn in turn_order:
+        crossing[turn] = part(2 * lax.rem(group + turn, 2) + other).astype(jnp.bfloat16)
+        cross(turn).start()
+    for turn in turn_order:
+        own_ref[turn] = part(2 * lax.rem(group + turn, 2) + half)
+
+    def home(turn, step):
+        return remote(
+            final.at[turn, rows_of(peer(step))],
+            back.at[group, rows_of(me)],
+            home_send.at[turn, step],
+            home_recv.at[turn, step],
+            {"ep": peer(step), "tp": 2 * lax.rem(group + turn, 2) + half},
+        )
+
+    for turn in turn_order:
+        cross(turn).wait_recv()
+        final[turn] = (own_ref[turn] + halves[turn].astype(jnp.float32)).astype(jnp.bfloat16)
+        for step in list(range(1, ep_count)) + ([0] if turn else []):
+            home(turn, step).start()
+    back[group, rows_of(me), :] = final[0, rows_of(me), :]
+
+    for n in (5, 8, 9, 10):
+        loads[n].wait()
+    state[...] = jnp.zeros_like(state)
+
+    def one(turn, _):
+        arrival(turn).wait_recv()
+        for p in range(pairs):
+            block = held[turn, p]
+            high, low = pair_parts(state[p], masks)
+            through = block[:, :wide]
+            state[p] = mm(
+                jnp.concatenate([through, through], axis=1), jnp.concatenate([high, low], axis=0)
+            ) + block[:, wide:].astype(jnp.float32)
+        return 0
+
+    lax.fori_loop(0, seat, one, 0)
+    ones_head = head_ones()
+    for p in range(pairs):
+        lanes = slice(p * wide, (p + 1) * wide)
+        block = part_map[p]
+        high, low = pair_parts(state[p], masks)
+        through = block[:, :wide]
+        moved = mm(
+            jnp.concatenate([through, through], axis=1), jnp.concatenate([high, low], axis=0)
+        ) + block[:, wide:].astype(jnp.float32)
+        current = jnp.where(side == 1, moved, state[p])
+        value = value_ref[:, lanes] + pair_dot(carry_ref[:, lanes], pair_parts(current, masks))
+        centred = value - head_sum(value, ones_head) * (1.0 / HEAD_CHANNELS)
+        spread = head_sum(centred * centred, ones_head) * (1.0 / HEAD_CHANNELS)
+        heads_ref[:, lanes] = (
+            centred
+            * lax.rsqrt(spread + GROUP_EPSILON)
+            * hgain_ref[:, lanes]
+            * jax.nn.sigmoid(gate_ref[:, lanes].astype(jnp.float32))
+        ).astype(jnp.bfloat16)
+    for j in range(4):
+        span = slice(j * columns, (j + 1) * columns)
+        made = mm(heads_ref[...], wout_ref[:, span]).astype(jnp.bfloat16)
+        for b in range(4):
+            mix[b, :, span] = made[b * block_rows : (b + 1) * block_rows]
+
+    def mix_cross(g):
+        return remote(
+            mix.at[2 * g + other],
+            mix_half.at[g],
+            mx_send.at[g],
+            mx_recv.at[g],
+            {"tp": partner},
+        )
+
+    for g in range(2):
+        mix_cross(g).start()
+    for g in range(2):
+        mix_cross(g).wait_recv()
+        mix_sum[g] = mix[2 * g + half].astype(jnp.float32) + mix_half[g].astype(jnp.float32)
+    mix_last[0] = mix_sum[1 - group].astype(jnp.bfloat16)
+    mix_tail = remote(
+        mix_last.at[0], mix_last.at[1], tail_send.at[1], tail_recv.at[1], {"tp": across}
+    )
+    mix_tail.start()
+
+    all_slots = 2 * slots
+    slot = lax.broadcasted_iota(jnp.int32, (experts, all_slots), 1)
+    which = lax.broadcasted_iota(jnp.int32, (experts, all_slots), 0)
+    holder = jnp.where(
+        which == 2 * ((slot % slots) // capacity) + slot // slots, 1.0, 0.0
+    ).astype(jnp.bfloat16)
+    slot_rank = (
+        lax.broadcasted_iota(jnp.int32, (tok_rows, all_slots), 1) % capacity
+    ).astype(jnp.float32)
+    hit = mm(rank, holder, TN) == slot_rank
+    weight_high, weight_low = split_parts(weight_of)
+    picks = [
+        jnp.where(hit, mm(w, holder, TN), 0.0).astype(jnp.bfloat16)
+        for w in (weight_high, weight_low)
+    ]
+    shared_tail.wait_recv()
+    base = shared_sum[group] + shared_last[1].astype(jnp.float32)
+    for turn in range(2):
+        for step in range(ep_count):
+            if step or turn:
+                home(turn, step).wait_recv()
+    returned = back[...].reshape(all_slots, columns)
+    routed = mm(
+        jnp.concatenate(picks, axis=1), jnp.concatenate([returned, returned], axis=0)
+    )
+    expert_out[...] = (routed + base).astype(jnp.bfloat16)
+
+    mix_tail.wait_recv()
+    total = mix_sum[group] + mix_last[1].astype(jnp.float32)
+    attn_out[...] = rms_scale(total, pgain_ref[...]).astype(jnp.bfloat16)
+
+    for step in order:
+        dispatch(step).wait_send()
+    for step in range(ep_count):
+        forward(step).wait_send()
+    swap.wait_send()
+    for step in range(1, seats):
+
+        @pl.when(seat + step < seats)
+        def _():
+            upward(step).wait_send()
+
+    for g in range(2):
+        shared_cross(g).wait_send()
+        cross(g).wait_send()
+        mix_cross(g).wait_send()
+    shared_tail.wait_send()
+    mix_tail.wait_send()
+    for turn in range(2):
+        for step in range(ep_count):
+            if step or turn:
+                home(turn, step).wait_send()
+
+
+def mega(
+    receptance, head_key_input, head_value_input, decay_input_part, learning_rate_input,
+    output_gate_input, decay_channel_offset, spike_log_decay, head_norm_gain, head_output_weight,
+    projection_norm_gain, expert_input_rows, expert_norm_gain, selected_expert_index,
+    selected_expert_weight, routed_gate_weight, routed_up_weight, routed_down_weight,
+    common_gate_weight, common_up_weight, common_down_weight,
+):
+    ep_count = lax.axis_size("ep")
+    rows, width = receptance.shape
+    tok_rows, model_width = expert_input_rows.shape
+    chosen = selected_expert_index.shape[1]
+    capacity = tok_rows * chosen // ep_count
+    slots = ep_count * capacity
+    columns = model_width // 4
+    wide = 2 * HEAD_CHANNELS
+    pairs = width // wide
+    operands = (
+        receptance, head_key_input, head_value_input, decay_input_part, learning_rate_input,
+        output_gate_input, decay_channel_offset[None, :], spike_log_decay, head_norm_gain[None, :],
+        head_output_weight, projection_norm_gain[None, :], expert_input_rows,
+        expert_norm_gain[None, :], selected_expert_index.T, selected_expert_weight.T,
+        routed_gate_weight[0], routed_up_weight[0], routed_down_weight[0], common_gate_weight,
+        common_up_weight, common_down_weight,
+    )
+    bf16, f32 = jnp.bfloat16, jnp.float32
+    dma = pltpu.SemaphoreType.DMA
+    scratch = [pltpu.VMEM(o.shape, o.dtype) for o in operands] + [
+        pltpu.VMEM((tok_rows, model_width), bf16),
+        pltpu.VMEM((slots, model_width // 2), bf16),
+        pltpu.VMEM((2, slots, model_width // 2), bf16),
+        pltpu.VMEM((rows, width), f32),
+        pltpu.VMEM((rows, width), f32),
+        pltpu.VMEM((pairs, HEAD_CHANNELS, 2 * wide), bf16),
+        pltpu.VMEM((pairs, HEAD_CHANNELS, 2 * wide), bf16),
+        pltpu.VMEM((pairs, HEAD_CHANNELS, 2 * wide), bf16),
+        pltpu.VMEM((ep_count // 2, pairs, HEAD_CHANNELS, 2 * wide), bf16),
+        pltpu.VMEM((pairs, HEAD_CHANNELS, wide), f32),
+        pltpu.VMEM((4, tok_rows, columns), bf16),
+        pltpu.VMEM((2, tok_rows, columns), bf16),
+        pltpu.VMEM((2, tok_rows, columns), f32),
+        pltpu.VMEM((2, tok_rows, columns), bf16),
+        pltpu.VMEM((2, slots, columns), bf16),
+        pltpu.VMEM((2, slots, columns), bf16),
+        pltpu.VMEM((2, slots, columns), f32),
+        pltpu.VMEM((2, slots, columns), bf16),
+        pltpu.VMEM((2, slots, columns), bf16),
+        pltpu.VMEM((rows, width), bf16),
+        pltpu.VMEM((4, rows // 4, model_width), bf16),
+        pltpu.VMEM((2, rows // 4, model_width), bf16),
+        pltpu.VMEM((2, rows // 4, model_width), f32),
+        pltpu.VMEM((2, rows // 4, model_width), bf16),
+        dma((len(operands),)),
+    ]
+    scratch += [dma((ep_count,))] * 4
+    scratch += [dma((1,))] * 2
+    scratch += [dma((ep_count // 2,))] * 2
+    scratch += [dma((2,))] * 4
+    scratch += [dma((2, ep_count))] * 2
+    scratch += [dma((2,))] * 4
+    full = pl.BlockSpec(memory_space=pltpu.VMEM)
+    return pl.pallas_call(
+        functools.partial(mega_kernel, ep_count),
+        out_shape=(
+            jax.ShapeDtypeStruct((rows // 4, model_width), bf16),
+            jax.ShapeDtypeStruct((tok_rows, columns), bf16),
+        ),
+        in_specs=[pl.BlockSpec(memory_space=pl.ANY)] * len(operands),
+        out_specs=(full, full),
+        scratch_shapes=scratch,
+        compiler_params=pltpu.CompilerParams(collective_id=0, has_side_effects=True),
+    )(*operands)
+
+
+def fits_mega(receptance, expert_input_rows, selected_expert_index):
+    ep_count = lax.axis_size("ep")
+    rows, width = receptance.shape
+    tok_rows, model_width = expert_input_rows.shape
+    assigned = tok_rows * selected_expert_index.shape[1]
+    return (
+        lax.axis_size("tp") == 4
+        and ep_count % 2 == 0
+        and width % (2 * HEAD_CHANNELS) == 0
+        and rows % (4 * BLOCK) == 0
+        and assigned % (16 * ep_count) == 0
+        and tok_rows % 128 == 0
+        and tok_rows <= 256
+        and model_width % 512 == 0
+    )
+
+
 def body(
     receptance,
     head_key_input,
@@ -504,6 +1171,14 @@
     common_up_weight,
     common_down_weight,
 ):
+    if fits_mega(receptance, expert_input_rows, selected_expert_index):
+        return mega(
+            receptance, head_key_input, head_value_input, decay_input_part, learning_rate_input,
+            output_gate_input, decay_channel_offset, spike_log_decay, head_norm_gain,
+            head_output_weight, projection_norm_gain, expert_input_rows, expert_norm_gain,
+            selected_expert_index, selected_expert_weight, routed_gate_weight, routed_up_weight,
+            routed_down_weight, common_gate_weight, common_up_weight, common_down_weight,
+        )
     attention_output = attention_mixer(
         receptance,
         head_key_input,

time: 105 us -> 43.8 us (0.42)
  the two profiles are of different devices: /device:TPU:0 before, /device:TPU:25 now
where the time goes in v1:
time: 43.8 us; the launch traced here: 43.7 us
  Pallas kernels  40.7 us (93%)
  local copies, waits for them, and re-layouts  2.36 us (5%)
  between operations  0.66 us (2%)
    pallas_call x1, Pallas kernels, mega(): pl.pallas_call(functools.partial(mega_kernel, ep_count), out_shape=(jax.S...  40.7 us
    unnamed x4, local copies, waits for them, and re-layouts  2.36 us

profile of v1, /device:TPU:25, one launch (start us, length us, event | category | flops | bytes accessed | tf_op | source)
XLA Modules:
  0.0 43.7 jit_solution(6025779638210361083)
XLA Ops:
  0.6 40.7 %shard_map.212 = (bf16[64,2048]{1,0:T(8,128)(2,1)}, bf16[128,512]{1,0:T(8,128)(2,1)}) custom-call(bf16[256,256]{1,0:T(8,128)(2,1)} %refs_0_.1, bf16[256,256]{1,0:T(8,128)(2,1)} %refs_1_.1, bf16[256,256]{1,0:T(8,128)(2,1)} %refs_2_.1, bf16[256,256]{1,0:T(8,128)(2,1)} %refs_3_.1, bf16[256,256]{1,0:T(8,128)(2,1)} %refs_4_.1, bf16[256,256]{1,0:T(8,128)(2,1)} %refs_5_.1, ...), custom_call_target="tpu_custom_call" | custom-call | tf_op jit(solution)/shard_map/pallas_call | solution.py:1121
  41.3 0.0 copy-start
  41.3 1.7 %copy.25 = bf16[64,2048]{1,0:T(8,128)(2,1)} copy(bf16[64,2048]{1,0:T(8,128)(2,1)} %get-tuple-element.4) | data formatting | bytes 524288
  43.0 0.0 copy-done
  43.0 0.7 %copy.26 = bf16[128,512]{1,0:T(8,128)(2,1)} copy(bf16[128,512]{1,0:T(8,128)(2,1)S(1)} %copy-done) | data formatting | bytes 262144
Async XLA Ops:
  41.3 1.7 %copy-start = (bf16[128,512]{1,0:T(8,128)(2,1)S(1)}, bf16[128,512]{1,0:T(8,128)(2,1)}, u32[]{:S(2)}) copy-start(bf16[128,512]{1,0:T(8,128)(2,1)} %get-tuple-element.5) | copy-start | bytes 393220

commit v2 on v1

--- a/solution.py
+++ b/solution.py
@@ -666,23 +666,30 @@
     return compact, finish
 
 
+def flipped_rows(index, bits, count):
+    result, unit = 0, 1
+    while unit < count:
+        digit = (index // unit) % 2
+        result = result + unit * ((digit + bits // unit) % 2)
+        unit *= 2
+    return result
+
+
 def mega_kernel(ep_count, *refs):
-    (
-        r_in, k_in, v_in, dec_in, lr_in, gate_in, off_in, spike_in, hgain_in, wout_in, pgain_in,
-        x_in, egain_in, idx_in, wsel_in, wg_in, wu_in, wd_in, cg_in, cu_in, cd_in,
-    ) = refs[:21]
+    inputs = refs[:21]
     attn_out, expert_out = refs[21:23]
+    copies = refs[23:44]
     (
         r_ref, k_ref, v_ref, dec_ref, lr_ref, gate_ref, off_ref, spike_ref, hgain_ref, wout_ref,
         pgain_ref, x_ref, egain_ref, idx_ref, wsel_ref, wg_ref, wu_ref, wd_ref, cg_ref, cu_ref,
         cd_ref,
-    ) = refs[23:44]
+    ) = copies
     (
-        normed, outgoing, arrived, carry_ref, value_ref, own_map, part_map, own_join, held, state,
-        shared, shared_half, shared_sum, shared_last, crossing, halves, own_ref, final, back,
-        heads_ref, mix, mix_half, mix_sum, mix_last,
-        load_sem, disp_send, disp_recv, fwd_send, fwd_recv, map_send, map_recv, join_send,
-        join_recv, sh_send, sh_recv, cross_send, cross_recv, home_send, home_recv, mx_send,
+        normed, outgoing, arrived, carry_ref, value_ref, own_map, held, base_state, state,
+        next_state, shared, shared_half, shared_sum, shared_last, crossing,
+        halves, own_ref, final, back, heads_ref, mix, mix_half, mix_sum, mix_last,
+        load_sem, disp_send, disp_recv, fwd_send, fwd_recv, map_send, map_recv, base_send,
+        base_recv, sh_send, sh_recv, cross_send, cross_recv, home_send, home_recv, mx_send,
         mx_recv, tail_send, tail_recv,
     ) = refs[44:]
     me = lax.axis_index("ep")
@@ -692,9 +699,9 @@
     other = 1 - half
     partner = 2 * group + other
     across = 2 * (1 - group) + half
-    seat = me // 2
-    side = me % 2
-    seats = ep_count // 2
+    level = me // 4
+    member = me % 4
+    levels = ep_count // 4
     tok_rows, model_width = x_ref.shape
     slots = outgoing.shape[0]
     capacity = slots // ep_count
@@ -704,44 +711,44 @@
     wide = 2 * HEAD_CHANNELS
     pairs = width // wide
     block_rows = rows // 4
+    quarter = ep_count // 4
+    outer = (level + member // 2 + 1) % 2
+    first_start = quarter * (2 + outer)
+    second_start = quarter * (3 - outer)
+    first_batch = [first_start + n for n in range(quarter)]
+    second_batch = [second_start + n for n in range(quarter)]
+    near_batch = list(range(2 * quarter))
 
     barrier = pltpu.get_barrier_semaphore()
 
-    def peer(step):
-        return lax.rem(me + step, ep_count)
-
-    for step in range(ep_count):
+    def peer(bits):
+        return flipped_rows(me, bits, ep_count)
+
+    def tp_of(turn):
+        return 2 * lax.rem(group + turn, 2) + half
+
+    for bits in range(ep_count):
         for turn in range(2):
-            if step or turn:
+            if bits or turn:
                 pl.semaphore_signal(
                     barrier,
                     inc=1,
-                    device_id={
-                        "ep": peer(step),
-                        "tp": 2 * lax.rem(group + turn, 2) + half,
-                    },
+                    device_id={"ep": peer(bits), "tp": tp_of(turn)},
                     device_id_type=MESH,
                 )
     pl.semaphore_signal(barrier, inc=1, device_id={"tp": partner}, device_id_type=MESH)
 
-    sources = (
-        r_in, k_in, v_in, dec_in, lr_in, gate_in, off_in, spike_in, hgain_in, wout_in, pgain_in,
-        x_in, egain_in, idx_in, wsel_in, wg_in, wu_in, wd_in, cg_in, cu_in, cd_in,
-    )
-    targets = (
-        r_ref, k_ref, v_ref, dec_ref, lr_ref, gate_ref, off_ref, spike_ref, hgain_ref, wout_ref,
-        pgain_ref, x_ref, egain_ref, idx_ref, wsel_ref, wg_ref, wu_ref, wd_ref, cg_ref, cu_ref,
-        cd_ref,
-    )
     loads = [
         pltpu.make_async_copy(source, target, load_sem.at[n])
-        for n, (source, target) in enumerate(zip(sources, targets))
+        for n, (source, target) in enumerate(zip(inputs, copies))
     ]
     for n in (11, 12, 13, 14, 0, 1, 2, 3, 4, 6, 7, 18, 19, 20, 15, 16, 17, 5, 8, 9, 10):
         loads[n].start()
 
-    def rows_of(index):
-        return pl.ds(pl.multiple_of(index * capacity, capacity), capacity)
+    def rows_of(bits):
+        if isinstance(bits, int):
+            return slice(bits * capacity, (bits + 1) * capacity)
+        return pl.ds(pl.multiple_of(bits * capacity, capacity), capacity)
 
     def remote(source, target, send, recv, where):
         return pltpu.make_async_remote_copy(
@@ -753,22 +760,21 @@
             device_id_type=MESH,
         )
 
-    def dispatch(step):
+    def dispatch(bits):
         return remote(
-            outgoing.at[rows_of(peer(step))],
-            arrived.at[half, rows_of(me)],
-            disp_send.at[step],
-            disp_recv.at[step],
-            {"ep": peer(step)},
-        )
-
-    def forward(step):
-        came = lax.rem(me + ep_count - step, ep_count)
+            outgoing.at[rows_of(bits)],
+            arrived.at[half, rows_of(bits)],
+            disp_send.at[bits],
+            disp_recv.at[bits],
+            {"ep": peer(bits)},
+        )
+
+    def forward(bits):
         return remote(
-            arrived.at[half, rows_of(came)],
-            arrived.at[half, rows_of(came)],
-            fwd_send.at[step],
-            fwd_recv.at[step],
+            arrived.at[half, rows_of(bits)],
+            arrived.at[half, rows_of(bits)],
+            fwd_send.at[bits],
+            fwd_recv.at[bits],
             {"tp": partner},
         )
 
@@ -779,7 +785,7 @@
     experts = 2 * ep_count
     expert_row = lax.broadcasted_iota(jnp.int32, (experts, tok_rows), 0)
     named = [expert_row == idx_ref[k : k + 1, :] for k in range(chosen_count)]
-    member = functools.reduce(jnp.logical_or, named)
+    chosen = functools.reduce(jnp.logical_or, named)
     weight_of = functools.reduce(
         jnp.add, [jnp.where(n, wsel_ref[k : k + 1, :], 0.0) for k, n in enumerate(named)]
     )
@@ -787,77 +793,73 @@
         jnp.int32, (tok_rows, tok_rows), 1
     )
     rank = mm(
-        jnp.where(member, 1.0, 0.0).astype(jnp.bfloat16),
+        jnp.where(chosen, 1.0, 0.0).astype(jnp.bfloat16),
         jnp.where(early, 1.0, 0.0).astype(jnp.bfloat16),
     )
-    rank = jnp.where(member, rank, -1.0).astype(jnp.bfloat16)
+    rank = jnp.where(chosen, rank, -1.0).astype(jnp.bfloat16)
     slot = lax.broadcasted_iota(jnp.int32, (slots, experts), 0)
     which = lax.broadcasted_iota(jnp.int32, (slots, experts), 1)
-    mine = jnp.where(which == 2 * (slot // capacity) + group, 1.0, 0.0).astype(jnp.bfloat16)
+    there = flipped_rows(me, slot // capacity, ep_count)
+    mine = jnp.where(which == 2 * there + group, 1.0, 0.0).astype(jnp.bfloat16)
     slot_rank = (
         lax.broadcasted_iota(jnp.int32, (slots, tok_rows), 0) % capacity
     ).astype(jnp.float32)
     placing = jnp.where(mm(mine, rank) == slot_rank, 1.0, 0.0).astype(jnp.bfloat16)
     fold_span = pl.ds(pl.multiple_of(half * fold, fold), fold)
+    other_span = pl.ds(pl.multiple_of(other * fold, fold), fold)
     outgoing[...] = mm(placing, normed[:, fold_span]).astype(jnp.bfloat16)
-    arrived[half, rows_of(me), :] = outgoing[rows_of(me), :]
     pl.semaphore_wait(barrier, 2 * ep_count)
-    order = list(range(1, ep_count))
-    for step in order:
-        dispatch(step).start()
-    forward(0).start()
+    order = list(range(2 * quarter, ep_count)) + near_batch[1:]
+    for bits in order[: 2 * quarter]:
+        dispatch(bits).start()
+
+    @pl.when(outer == 0)
+    def _():
+        for bits in order[2 * quarter :]:
+            dispatch(bits).start()
+
+    arrived[half, rows_of(0), :] = outgoing[rows_of(0), :]
+    arrived[other, rows_of(0), :] = mm(placing[:capacity], normed[:, other_span]).astype(
+        jnp.bfloat16
+    )
 
     for n in (0, 1, 2, 3, 4, 6, 7):
         loads[n].wait()
     compact, finish = local_math(r_ref, k_ref, v_ref, dec_ref, lr_ref, off_ref, spike_ref)
     for p in range(pairs):
         own_map[p] = compact[p].astype(jnp.bfloat16)
-    swap = remote(
-        own_map, part_map, map_send.at[0], map_recv.at[0], {"ep": 2 * seat + 1 - side}
-    )
-    swap.start()
+    masks = pair_masks()
+
+    def give(there):
+        return remote(
+            own_map,
+            held.at[member],
+            map_send.at[there],
+            map_recv.at[member],
+            {"ep": 4 * level + there},
+        )
+
+    def taken(source):
+        return remote(
+            own_map, held.at[source], map_send.at[0], map_recv.at[source], {"ep": peer(1)}
+        )
+
+    def gives(there):
+        above_me = member < there
+        return above_me | (member == 3) if there == 2 else above_me
+
+    for there in (3, 2, 1):
+
+        @pl.when(gives(there))
+        def _():
+            give(there).start()
+
     for (i, p), (carry, value) in finish().items():
         span = slice(i * BLOCK, (i + 1) * BLOCK)
         lanes = slice(p * wide, (p + 1) * wide)
         carry_ref[span, lanes] = carry
         value_ref[span, lanes] = value
 
-    masks = pair_masks()
-    swap.wait_recv()
-    for p in range(pairs):
-        mine_map = own_map[p]
-        their_map = part_map[p]
-        first = jnp.where(side == 0, mine_map, their_map)
-        second = jnp.where(side == 0, their_map, mine_map)
-        blocks = jnp.concatenate(
-            [stacked(first[:, :wide], masks), stacked(first[:, wide:], masks)], axis=1
-        )
-        joined = mm(second[:, :wide], blocks)
-        own_join[p] = jnp.concatenate(
-            [joined[:, :wide], joined[:, wide:] + second[:, wide:].astype(jnp.float32)], axis=1
-        ).astype(jnp.bfloat16)
-
-    def upward(step):
-        return remote(
-            own_join,
-            held.at[seat],
-            join_send.at[step],
-            join_recv.at[seat],
-            {"ep": lax.rem(me + 2 * step, ep_count)},
-        )
-
-    def arrival(turn):
-        return remote(
-            own_join, held.at[turn], join_send.at[1], join_recv.at[turn],
-            {"ep": lax.rem(me + 2, ep_count)},
-        )
-
-    for step in range(1, seats):
-
-        @pl.when(seat + step < seats)
-        def _():
-            upward(step).start()
-
     for n in (18, 19, 20):
         loads[n].wait()
     rows_in = normed[...]
@@ -867,149 +869,246 @@
     for j in range(4):
         shared[j] = mm(hidden, cd_ref[:, j * columns : (j + 1) * columns]).astype(jnp.bfloat16)
 
-    def shared_cross(g):
+    def shared_cross(turn):
+        there = 2 * lax.rem(group + turn, 2) + other
         return remote(
-            shared.at[2 * g + other],
-            shared_half.at[g],
-            sh_send.at[g],
-            sh_recv.at[g],
+            shared.at[there],
+            shared_half.at[turn],
+            sh_send.at[turn],
+            sh_recv.at[turn],
             {"tp": partner},
         )
 
-    for g in range(2):
-        shared_cross(g).start()
+    for turn in (1, 0):
+        shared_cross(turn).start()
+
+    def take_in(batch):
+        for bits in batch:
+            if not isinstance(bits, int) or bits:
+                dispatch(bits).wait_recv()
+                forward(bits).start()
+
+    take_in(first_batch)
+
+    @pl.when(outer == 1)
+    def _():
+        for bits in order[2 * quarter :]:
+            dispatch(bits).start()
+
+    def wait_far(batch):
+        for bits in batch:
+            if not isinstance(bits, int) or bits:
+                forward(bits).wait_recv()
+
+    def cross(batch_index, turn, span):
+        return remote(
+            crossing.at[turn, span],
+            halves.at[turn, span],
+            cross_send.at[batch_index, turn],
+            cross_recv.at[batch_index, turn],
+            {"tp": partner},
+        )
+
+    def home(turn, bits):
+        return remote(
+            final.at[turn, rows_of(bits)],
+            back.at[group, rows_of(bits)],
+            home_send.at[turn, bits],
+            home_recv.at[turn, bits],
+            {"ep": peer(bits), "tp": tp_of(turn)},
+        )
+
+    def span_of(batch):
+        if isinstance(batch[0], int):
+            return slice(0, len(batch) * capacity)
+        size = quarter * capacity
+        return pl.ds(pl.multiple_of(batch[0] * capacity, size), size)
+
+    def feed(batch_index, batch):
+        span = span_of(batch)
+        near, away = arrived[0, span, :], arrived[1, span, :]
+        gate = mm(near, wg_ref[:fold, :]) + mm(away, wg_ref[fold:, :])
+        upper = mm(near, wu_ref[:fold, :]) + mm(away, wu_ref[fold:, :])
+        routed_hidden = (jax.nn.silu(gate) * upper).astype(jnp.bfloat16)
+
+        def part(index):
+            lanes = pl.ds(pl.multiple_of(index * columns, columns), columns)
+            return mm(routed_hidden, wd_ref[:, lanes])
+
+        for turn in (1, 0):
+            crossing[turn, span, :] = part(2 * lax.rem(group + turn, 2) + other).astype(
+                jnp.bfloat16
+            )
+            cross(batch_index, turn, span).start()
+        for turn in (1, 0):
+            own_ref[turn, span, :] = part(2 * lax.rem(group + turn, 2) + half)
+
+    def send_home(batch_index, batch):
+        span = span_of(batch)
+        for turn in (1, 0):
+            cross(batch_index, turn, span).wait_recv()
+            final[turn, span, :] = (
+                own_ref[turn, span, :] + halves[turn, span, :].astype(jnp.float32)
+            ).astype(jnp.bfloat16)
+            for bits in batch:
+                if not isinstance(bits, int) or bits or turn:
+                    home(turn, bits).start()
+                else:
+                    back[group, rows_of(0), :] = final[0, rows_of(0), :]
 
     for n in (15, 16, 17):
         loads[n].wait()
-    for step in order:
-        dispatch(step).wait_recv()
-        forward(step).start()
-    other_span = pl.ds(pl.multiple_of(other * fold, fold), fold)
-    own_rows = arrived[half]
-    gate = mm(own_rows, wg_ref[fold_span, :])
-    upper = mm(own_rows, wu_ref[fold_span, :])
-
-    for g in range(2):
-        shared_cross(g).wait_recv()
-        shared_sum[g] = shared[2 * g + half].astype(jnp.float32) + shared_half[g].astype(
+    wait_far(first_batch)
+    feed(0, first_batch)
+    for turn in (1, 0):
+        shared_cross(turn).wait_recv()
+        shared_sum[turn] = shared[tp_of(turn)].astype(jnp.float32) + shared_half[turn].astype(
             jnp.float32
         )
-    shared_last[0] = shared_sum[1 - group].astype(jnp.bfloat16)
+    shared_last[0] = shared_sum[1].astype(jnp.bfloat16)
     shared_tail = remote(
         shared_last.at[0], shared_last.at[1], tail_send.at[0], tail_recv.at[0], {"tp": across}
     )
     shared_tail.start()
-
-    for step in range(ep_count):
-        forward(step).wait_recv()
-    other_rows = arrived[other]
-    gate = gate + mm(other_rows, wg_ref[other_span, :])
-    upper = upper + mm(other_rows, wu_ref[other_span, :])
-    routed_hidden = (jax.nn.silu(gate) * upper).astype(jnp.bfloat16)
-
-    def part(index):
-        span = pl.ds(pl.multiple_of(index * columns, columns), columns)
-        return mm(routed_hidden, wd_ref[:, span])
-
-    def cross(turn):
+    def moved_by(block, p, current):
+        through = block[p, :, :wide]
+        high, low = pair_parts(current, masks)
+        return mm(
+            jnp.concatenate([through, through], axis=1), jnp.concatenate([high, low], axis=0)
+        ) + block[p, :, wide:].astype(jnp.float32)
+
+    def above(turn):
         return remote(
-            crossing.at[turn],
-            halves.at[turn],
-            cross_send.at[turn],
-            cross_recv.at[turn],
-            {"tp": partner},
-        )
-
-    turn_order = (1, 0)
-    for turn in turn_order:
-        crossing[turn] = part(2 * lax.rem(group + turn, 2) + other).astype(jnp.bfloat16)
-        cross(turn).start()
-    for turn in turn_order:
-        own_ref[turn] = part(2 * lax.rem(group + turn, 2) + half)
-
-    def home(turn, step):
-        return remote(
-            final.at[turn, rows_of(peer(step))],
-            back.at[group, rows_of(me)],
-            home_send.at[turn, step],
-            home_recv.at[turn, step],
-            {"ep": peer(step), "tp": 2 * lax.rem(group + turn, 2) + half},
-        )
-
-    for turn in turn_order:
-        cross(turn).wait_recv()
-        final[turn] = (own_ref[turn] + halves[turn].astype(jnp.float32)).astype(jnp.bfloat16)
-        for step in list(range(1, ep_count)) + ([0] if turn else []):
-            home(turn, step).start()
-    back[group, rows_of(me), :] = final[0, rows_of(me), :]
-
+            next_state,
+            base_state,
+            base_send.at[turn],
+            base_recv.at[0],
+            {"ep": lax.rem(4 * (level + 1) + 2 * turn + member % 2, ep_count)},
+        )
+
+    hands_on = (member >= 2) & (level + 1 < levels)
+
+    def settle():
+        for p in range(pairs):
+            state[p] = base_state[p].astype(jnp.float32)
+        for source in range(3):
+
+            @pl.when(source < member)
+            def _():
+                taken(source).wait_recv()
+                for p in range(pairs):
+                    state[p] = moved_by(held.at[source], p, state[p])
+
+        @pl.when(member == 2)
+        def _():
+            taken(3).wait_recv()
+
+        @pl.when(hands_on)
+        def _():
+            for p in range(pairs):
+                once = moved_by(own_map, p, state[p])
+                twice = moved_by(held.at[3], p, once)
+                next_state[p] = jnp.where(member == 2, twice, once).astype(jnp.bfloat16)
+            for turn in range(2):
+                above(turn).start()
+
+    @pl.when(level == 0)
+    def _():
+        base_state[...] = jnp.zeros_like(base_state)
+        settle()
+
+    send_home(0, first_batch)
     for n in (5, 8, 9, 10):
         loads[n].wait()
-    state[...] = jnp.zeros_like(state)
-
-    def one(turn, _):
-        arrival(turn).wait_recv()
+
+    def mix_cross(turn):
+        there = 2 * lax.rem(group + turn, 2) + other
+        return remote(
+            mix.at[there],
+            mix_half.at[turn],
+            mx_send.at[turn],
+            mx_recv.at[turn],
+            {"tp": partner},
+        )
+
+    def project(turn):
+        there = lax.rem(group + turn, 2)
+        rows_there = pl.ds(pl.multiple_of(there * 2 * block_rows, 2 * block_rows), 2 * block_rows)
+        rows_made = heads_ref[rows_there, :]
+        for j in range(4):
+            span = slice(j * columns, (j + 1) * columns)
+            made = mm(rows_made, wout_ref[:, span]).astype(jnp.bfloat16)
+            for b in range(2):
+                mix[2 * there + b, :, span] = made[b * block_rows : (b + 1) * block_rows]
+
+    def attend():
+        ones_head = head_ones()
         for p in range(pairs):
-            block = held[turn, p]
-            high, low = pair_parts(state[p], masks)
-            through = block[:, :wide]
-            state[p] = mm(
-                jnp.concatenate([through, through], axis=1), jnp.concatenate([high, low], axis=0)
-            ) + block[:, wide:].astype(jnp.float32)
-        return 0
-
-    lax.fori_loop(0, seat, one, 0)
-    ones_head = head_ones()
-    for p in range(pairs):
-        lanes = slice(p * wide, (p + 1) * wide)
-        block = part_map[p]
-        high, low = pair_parts(state[p], masks)
-        through = block[:, :wide]
-        moved = mm(
-            jnp.concatenate([through, through], axis=1), jnp.concatenate([high, low], axis=0)
-        ) + block[:, wide:].astype(jnp.float32)
-        current = jnp.where(side == 1, moved, state[p])
-        value = value_ref[:, lanes] + pair_dot(carry_ref[:, lanes], pair_parts(current, masks))
-        centred = value - head_sum(value, ones_head) * (1.0 / HEAD_CHANNELS)
-        spread = head_sum(centred * centred, ones_head) * (1.0 / HEAD_CHANNELS)
-        heads_ref[:, lanes] = (
-            centred
-            * lax.rsqrt(spread + GROUP_EPSILON)
-            * hgain_ref[:, lanes]
-            * jax.nn.sigmoid(gate_ref[:, lanes].astype(jnp.float32))
-        ).astype(jnp.bfloat16)
-    for j in range(4):
-        span = slice(j * columns, (j + 1) * columns)
-        made = mm(heads_ref[...], wout_ref[:, span]).astype(jnp.bfloat16)
-        for b in range(4):
-            mix[b, :, span] = made[b * block_rows : (b + 1) * block_rows]
-
-    def mix_cross(g):
-        return remote(
-            mix.at[2 * g + other],
-            mix_half.at[g],
-            mx_send.at[g],
-            mx_recv.at[g],
-            {"tp": partner},
-        )
-
-    for g in range(2):
-        mix_cross(g).start()
-    for g in range(2):
-        mix_cross(g).wait_recv()
-        mix_sum[g] = mix[2 * g + half].astype(jnp.float32) + mix_half[g].astype(jnp.float32)
-    mix_last[0] = mix_sum[1 - group].astype(jnp.bfloat16)
+            lanes = slice(p * wide, (p + 1) * wide)
+            value = value_ref[:, lanes] + pair_dot(
+                carry_ref[:, lanes], pair_parts(state[p], masks)
+            )
+            centred = value - head_sum(value, ones_head) * (1.0 / HEAD_CHANNELS)
+            spread = head_sum(centred * centred, ones_head) * (1.0 / HEAD_CHANNELS)
+            heads_ref[:, lanes] = (
+                centred
+                * lax.rsqrt(spread + GROUP_EPSILON)
+                * hgain_ref[:, lanes]
+                * jax.nn.sigmoid(gate_ref[:, lanes].astype(jnp.float32))
+            ).astype(jnp.bfloat16)
+        for turn in (1, 0):
+            project(turn)
+            mix_cross(turn).start()
+
     mix_tail = remote(
         mix_last.at[0], mix_last.at[1], tail_send.at[1], tail_recv.at[1], {"tp": across}
     )
-    mix_tail.start()
+
+    def pass_mix():
+        mix_cross(1).wait_recv()
+        mix_last[0] = (
+            mix[across].astype(jnp.float32) + mix_half[1].astype(jnp.float32)
+        ).astype(jnp.bfloat16)
+        mix_tail.start()
+
+    @pl.when(level == 0)
+    def _():
+        attend()
+
+    take_in(near_batch)
+    wait_far(near_batch)
+    @pl.when(level == 0)
+    def _():
+        pass_mix()
+
+    feed(1, near_batch)
+    take_in(second_batch)
+    send_home(1, near_batch)
+
+    @pl.when(level > 0)
+    def _():
+        above(0).wait_recv()
+        settle()
+
+    @pl.when(level > 0)
+    def _():
+        attend()
+
+    wait_far(second_batch)
+    feed(2, second_batch)
+    @pl.when(level > 0)
+    def _():
+        pass_mix()
+
+    send_home(2, second_batch)
+    mix_cross(0).wait_recv()
+    mix_sum[...] = mix[place].astype(jnp.float32) + mix_half[0].astype(jnp.float32)
 
     all_slots = 2 * slots
     slot = lax.broadcasted_iota(jnp.int32, (experts, all_slots), 1)
     which = lax.broadcasted_iota(jnp.int32, (experts, all_slots), 0)
-    holder = jnp.where(
-        which == 2 * ((slot % slots) // capacity) + slot // slots, 1.0, 0.0
-    ).astype(jnp.bfloat16)
+    there = flipped_rows(me, (slot % slots) // capacity, ep_count)
+    holder = jnp.where(which == 2 * there + slot // slots, 1.0, 0.0).astype(jnp.bfloat16)
     slot_rank = (
         lax.broadcasted_iota(jnp.int32, (tok_rows, all_slots), 1) % capacity
     ).astype(jnp.float32)
@@ -1020,11 +1119,12 @@
         for w in (weight_high, weight_low)
     ]
     shared_tail.wait_recv()
-    base = shared_sum[group] + shared_last[1].astype(jnp.float32)
-    for turn in range(2):
-        for step in range(ep_count):
-            if step or turn:
-                home(turn, step).wait_recv()
+    base = shared_sum[0] + shared_last[1].astype(jnp.float32)
+    for batch in (first_batch, near_batch, second_batch):
+        for turn in range(2):
+            for bits in batch:
+                if not isinstance(bits, int) or bits or turn:
+                    home(turn, bits).wait_recv()
     returned = back[...].reshape(all_slots, columns)
     routed = mm(
         jnp.concatenate(picks, axis=1), jnp.concatenate([returned, returned], axis=0)
@@ -1032,30 +1132,33 @@
     expert_out[...] = (routed + base).astype(jnp.bfloat16)
 
     mix_tail.wait_recv()
-    total = mix_sum[group] + mix_last[1].astype(jnp.float32)
+    total = mix_sum[...] + mix_last[1].astype(jnp.float32)
     attn_out[...] = rms_scale(total, pgain_ref[...]).astype(jnp.bfloat16)
 
-    for step in order:
-        dispatch(step).wait_send()
-    for step in range(ep_count):
-        forward(step).wait_send()
-    swap.wait_send()
-    for step in range(1, seats):
-
-        @pl.when(seat + step < seats)
+    for bits in order:
+        dispatch(bits).wait_send()
+        forward(bits).wait_send()
+    for there in (3, 2, 1):
+
+        @pl.when(gives(there))
         def _():
-            upward(step).wait_send()
-
-    for g in range(2):
-        shared_cross(g).wait_send()
-        cross(g).wait_send()
-        mix_cross(g).wait_send()
+            give(there).wait_send()
+
+    @pl.when(hands_on)
+    def _():
+        for turn in range(2):
+            above(turn).wait_send()
+
+    for turn in range(2):
+        shared_cross(turn).wait_send()
+        mix_cross(turn).wait_send()
+        for n, batch in enumerate((first_batch, near_batch, second_batch)):
+            cross(n, turn, span_of(batch)).wait_send()
+        for bits in range(ep_count):
+            if bits or turn:
+                home(turn, bits).wait_send()
     shared_tail.wait_send()
     mix_tail.wait_send()
-    for turn in range(2):
-        for step in range(ep_count):
-            if step or turn:
-                home(turn, step).wait_send()
 
 
 def mega(
@@ -1091,10 +1194,10 @@
         pltpu.VMEM((rows, width), f32),
         pltpu.VMEM((rows, width), f32),
         pltpu.VMEM((pairs, HEAD_CHANNELS, 2 * wide), bf16),
-        pltpu.VMEM((pairs, HEAD_CHANNELS, 2 * wide), bf16),
-        pltpu.VMEM((pairs, HEAD_CHANNELS, 2 * wide), bf16),
-        pltpu.VMEM((ep_count // 2, pairs, HEAD_CHANNELS, 2 * wide), bf16),
+        pltpu.VMEM((4, pairs, HEAD_CHANNELS, 2 * wide), bf16),
+        pltpu.VMEM((pairs, HEAD_CHANNELS, wide), bf16),
         pltpu.VMEM((pairs, HEAD_CHANNELS, wide), f32),
+        pltpu.VMEM((pairs, HEAD_CHANNELS, wide), bf16),
         pltpu.VMEM((4, tok_rows, columns), bf16),
         pltpu.VMEM((2, tok_rows, columns), bf16),
         pltpu.VMEM((2, tok_rows, columns), f32),
@@ -1107,14 +1210,14 @@
         pltpu.VMEM((rows, width), bf16),
         pltpu.VMEM((4, rows // 4, model_width), bf16),
         pltpu.VMEM((2, rows // 4, model_width), bf16),
-        pltpu.VMEM((2, rows // 4, model_width), f32),
+        pltpu.VMEM((rows // 4, model_width), f32),
         pltpu.VMEM((2, rows // 4, model_width), bf16),
         dma((len(operands),)),
     ]
     scratch += [dma((ep_count,))] * 4
-    scratch += [dma((1,))] * 2
-    scratch += [dma((ep_count // 2,))] * 2
+    scratch += [dma((4,))] * 2
     scratch += [dma((2,))] * 4
+    scratch += [dma((3, 2))] * 2
     scratch += [dma((2, ep_count))] * 2
     scratch += [dma((2,))] * 4
     full = pl.BlockSpec(memory_space=pltpu.VMEM)
@@ -1138,7 +1241,8 @@
     assigned = tok_rows * selected_expert_index.shape[1]
     return (
         lax.axis_size("tp") == 4
-        and ep_count % 2 == 0
+        and ep_count >= 4
+        and ep_count & (ep_count - 1) == 0
         and width % (2 * HEAD_CHANNELS) == 0
         and rows % (4 * BLOCK) == 0
         and assigned % (16 * ep_count) == 0

time: 43.8 us -> 38.9 us (0.89)
  the two profiles are of different devices: /device:TPU:25 before, /device:TPU:17 now
where the time goes in v2:
time: 38.9 us; the launch traced here: 38.6 us
  Pallas kernels  35.6 us (92%)
  local copies, waits for them, and re-layouts  2.36 us (6%)
  between operations  0.66 us (2%)
    pallas_call x1, Pallas kernels, mega(): pl.pallas_call(functools.partial(mega_kernel, ep_count), out_shape=(jax.S...  35.6 us
    unnamed x4, local copies, waits for them, and re-layouts  2.36 us

profile of v2, /device:TPU:17, one launch (start us, length us, event | category | flops | bytes accessed | tf_op | source)
XLA Modules:
  0.0 38.6 jit_solution(14669428270731258528)
XLA Ops:
  0.6 35.6 %shard_map.212 = (bf16[64,2048]{1,0:T(8,128)(2,1)}, bf16[128,512]{1,0:T(8,128)(2,1)}) custom-call(bf16[256,256]{1,0:T(8,128)(2,1)} %refs_0_.1, bf16[256,256]{1,0:T(8,128)(2,1)} %refs_1_.1, bf16[256,256]{1,0:T(8,128)(2,1)} %refs_2_.1, bf16[256,256]{1,0:T(8,128)(2,1)} %refs_3_.1, bf16[256,256]{1,0:T(8,128)(2,1)} %refs_4_.1, bf16[256,256]{1,0:T(8,128)(2,1)} %refs_5_.1, ...), custom_call_target="tpu_custom_call" | custom-call | tf_op jit(solution)/shard_map/pallas_call | solution.py:1224
  36.3 0.0 copy-start
  36.3 1.7 %copy.25 = bf16[64,2048]{1,0:T(8,128)(2,1)} copy(bf16[64,2048]{1,0:T(8,128)(2,1)} %get-tuple-element.4) | data formatting | bytes 524288
  38.0 0.0 copy-done
  38.0 0.7 %copy.26 = bf16[128,512]{1,0:T(8,128)(2,1)} copy(bf16[128,512]{1,0:T(8,128)(2,1)S(1)} %copy-done) | data formatting | bytes 262144
Async XLA Ops:
  36.3 1.7 %copy-start = (bf16[128,512]{1,0:T(8,128)(2,1)S(1)}, bf16[128,512]{1,0:T(8,128)(2,1)}, u32[]{:S(2)}) copy-start(bf16[128,512]{1,0:T(8,128)(2,1)} %get-tuple-element.5) | copy-start | bytes 393220

commit v3 on v2

--- a/solution.py
+++ b/solution.py
@@ -503,6 +503,10 @@
     )
 
 
+def short_dot(x, y, masks):
+    return mm(x.astype(jnp.bfloat16), stacked(y.astype(jnp.bfloat16), masks))
+
+
 def pair_parts(y, masks):
     yh, yl = split_parts(y)
     return stacked(yh, masks), stacked(yl, masks)
@@ -541,59 +545,78 @@
     running = jnp.where((tcol % BLOCK <= trow) & (tcol < 3 * BLOCK), 1.0, 0.0).astype(jnp.bfloat16)
     blank = jnp.zeros((BLOCK, wide), jnp.bfloat16)
     items = [(i, p) for i in range(chunks) for p in range(pairs)]
-    lows, low_vs, out_bs, out_vs, ins_ends, b_ends, r_outs, a_ins, vs, ends = (
-        [] for _ in range(10)
-    )
+    spans = [slice(i * BLOCK, (i + 1) * BLOCK) for i in range(chunks)]
+    strips = [slice(p * wide, (p + 1) * wide) for p in range(pairs)]
+    pre = off_ref[...] + jnp.tanh(dec_ref[...].astype(jnp.float32))
+    log = spike_ref[...] - jax.nn.sigmoid(pre) * jnp.exp(jnp.float32(-0.5))
+    p0 = log.astype(jnp.bfloat16)
+    rest = log - p0.astype(jnp.float32)
+    p1 = rest.astype(jnp.bfloat16)
+    p2 = (rest - p1.astype(jnp.float32)).astype(jnp.bfloat16)
+    empty = jnp.zeros((BLOCK, width), jnp.bfloat16)
+    cums = [
+        mm(running, jnp.concatenate([p0[span], p1[span], p2[span], empty], axis=0))
+        for span in spans
+    ]
+    k_all = k_ref[...].astype(jnp.float32)
+    squares = k_all * k_all
+    sums = [head_sum(squares[:, strip], ones_head) for strip in strips]
+    learn = jax.nn.sigmoid(lr_ref[...].astype(jnp.float32))
+    scale = jnp.concatenate([lax.rsqrt(q + NORM_EPSILON) for q in sums], axis=1)
+    cum_all = jnp.concatenate(cums, axis=0)
+    back = learn * k_all * jnp.exp(-cum_all)
+    b_all = back * scale
+    a_all = k_all * scale * jnp.exp(cum_all - log)
+    r_all = r_ref[...].astype(jnp.float32) * jnp.exp(cum_all)
+    bh_all, bl_all = split_parts(b_all)
+    ih_all, il_all = split_parts(back)
+    ah_all, al_all = split_parts(a_all)
+    rh_all, rl_all = split_parts(r_all)
+    chunk_ends = [jnp.exp(c[BLOCK - 1 :]) for c in cums]
+    grams = []
     for i, p in items:
-        span = slice(i * BLOCK, (i + 1) * BLOCK)
-        lanes = slice(p * wide, (p + 1) * wide)
-        r = r_ref[span, lanes].astype(jnp.float32)
-        k = k_ref[span, lanes].astype(jnp.float32)
-        v = v_ref[span, lanes]
-        learn = jax.nn.sigmoid(lr_ref[span, lanes].astype(jnp.float32))
-        pre = off_ref[:, lanes] + jnp.tanh(dec_ref[span, lanes].astype(jnp.float32))
-        log = spike_ref[span, lanes] - jax.nn.sigmoid(pre) * jnp.exp(jnp.float32(-0.5))
-        p0 = log.astype(jnp.bfloat16)
-        rest = log - p0.astype(jnp.float32)
-        p1 = rest.astype(jnp.bfloat16)
-        p2 = (rest - p1.astype(jnp.float32)).astype(jnp.bfloat16)
-        cum = mm(running, jnp.concatenate([p0, p1, p2, blank], axis=0))
-        before = cum - log
-        last = cum[BLOCK - 1 :]
-        a = k * lax.rsqrt(head_sum(k * k, ones_head) + NORM_EPSILON)
-        back = jnp.exp(-cum)
-        end = jnp.exp(last)
-        a_in = a * jnp.exp(before)
-        r_out = r * jnp.exp(cum)
-        b_back = a * learn * back
-        ins_back = k * learn * back
-        lh, ll = split_parts(jnp.concatenate([a_in, r_out], axis=0))
-        bh, bl = split_parts(b_back)
-        ih, il = split_parts(ins_back)
-        right_high = jnp.concatenate([stacked(bh, masks), stacked(ih, masks)], axis=0)
-        right_low = jnp.concatenate([stacked(bl, masks), stacked(il, masks)], axis=0)
-        gram = mm(
-            jnp.concatenate([lh, ll], axis=1),
-            jnp.concatenate([right_high, right_high], axis=1),
-            NT,
-        ) + mm(lh, right_low, NT)
-        lows.append(jnp.where(strict, gram[:BLOCK, :wide], 0.0))
-        low_k = jnp.where(strict, gram[:BLOCK, wide:], 0.0)
-        out_bs.append(jnp.where(inclusive, gram[BLOCK:, :wide], 0.0))
-        out_k = jnp.where(inclusive, gram[BLOCK:, wide:], 0.0)
-        kh, kl = split_parts(jnp.concatenate([low_k, out_k], axis=0))
-        values = stacked(v, masks)
-        weighted = mm(
-            jnp.concatenate([kh, kl], axis=1), jnp.concatenate([values, values], axis=0)
-        )
-        low_vs.append(weighted[:BLOCK])
-        out_vs.append(weighted[BLOCK:])
-        ins_ends.append(ins_back * end)
-        b_ends.append(b_back * end)
-        r_outs.append(r_out)
-        a_ins.append(a_in)
-        vs.append(v)
-        ends.append(end)
+        at = (spans[i], strips[p])
+        left_high = jnp.concatenate([ah_all[at], rh_all[at]], axis=0)
+        left_low = jnp.concatenate([al_all[at], rl_all[at]], axis=0)
+        right_high = jnp.concatenate(
+            [stacked(bh_all[at], masks), stacked(ih_all[at], masks)], axis=0
+        )
+        right_low = jnp.concatenate(
+            [stacked(bl_all[at], masks), stacked(il_all[at], masks)], axis=0
+        )
+        grams.append(
+            mm(
+                jnp.concatenate([left_high, left_low], axis=1),
+                jnp.concatenate([right_high, right_high], axis=1),
+                NT,
+            )
+            + mm(left_high, right_low, NT)
+        )
+    lows = [jnp.where(strict, gram[:BLOCK, :wide], 0.0) for gram in grams]
+    out_bs = [jnp.where(inclusive, gram[BLOCK:, :wide], 0.0) for gram in grams]
+    vs = [v_ref[spans[i], strips[p]] for i, p in items]
+    weighted = []
+    for n, gram in enumerate(grams):
+        kh, kl = split_parts(
+            jnp.concatenate(
+                [
+                    jnp.where(strict, gram[:BLOCK, wide:], 0.0),
+                    jnp.where(inclusive, gram[BLOCK:, wide:], 0.0),
+                ],
+                axis=0,
+            )
+        )
+        values = stacked(vs[n], masks)
+        weighted.append(
+            mm(jnp.concatenate([kh, kl], axis=1), jnp.concatenate([values, values], axis=0))
+        )
+    low_vs = [w[:BLOCK] for w in weighted]
+    out_vs = [w[BLOCK:] for w in weighted]
+    ends = [chunk_ends[i][:, strips[p]] for i, p in items]
+    ins_ends = [back[spans[i], strips[p]] * ends[n] for n, (i, p) in enumerate(items)]
+    b_ends = [b_all[spans[i], strips[p]] * ends[n] for n, (i, p) in enumerate(items)]
+    r_outs = [r_all[spans[i], strips[p]] for i, p in items]
+    a_ins = [a_all[spans[i], strips[p]] for i, p in items]
     count = range(len(items))
     eye = jnp.where(row == col, 1.0, 0.0)
     inverses = None
@@ -604,12 +627,20 @@
         if size == 1:
             inverses = [eye - corner for corner in corners]
         else:
+            exact = 2 * size >= BLOCK
             firsts = [
-                pair_dot(inverses[n], pair_parts(corners[n], masks)) for n in count
+                pair_dot(inverses[n], pair_parts(corners[n], masks))
+                if exact
+                else short_dot(inverses[n], corners[n], masks)
+                for n in count
             ]
-            inverses = [
-                inverses[n] - pair_dot(firsts[n], pair_parts(inverses[n], masks)) for n in count
+            changes = [
+                pair_dot(firsts[n], pair_parts(inverses[n], masks))
+                if exact
+                else short_dot(firsts[n], inverses[n], masks)
+                for n in count
             ]
+            inverses = [inverses[n] - changes[n] for n in count]
         size *= 2
     solved = [
         side_by_side(pair_parts(a_ins[n], masks), pair_parts(low_vs[n], masks)) for n in count
@@ -631,18 +662,33 @@
         ) + mm(lh, low, TN)
         end = jnp.concatenate([ends[n], ends[n]], axis=1)
         maps.append(jnp.where(same_head, made + jnp.where(diagonal, end, 0.0), 0.0))
-    whole = [None] * pairs
-    heads_at = []
-    for n in count:
-        p = items[n][1]
-        heads_at.append(whole[p])
-        if whole[p] is None:
-            whole[p] = maps[n]
-        else:
-            joined = pair_dot(maps[n][:, :wide], split_parts(whole[p]))
-            whole[p] = jnp.concatenate(
-                [joined[:, :wide], joined[:, wide:] + maps[n][:, wide:]], axis=1
-            )
+    def after(second, first):
+        joined = pair_dot(second[:, :wide], split_parts(first))
+        return jnp.concatenate([joined[:, :wide], joined[:, wide:] + second[:, wide:]], axis=1)
+
+    by_pair = [maps[p::pairs] for p in range(pairs)]
+    stage = [list(row) for row in by_pair]
+    tree = [stage]
+    while len(stage[0]) > 1:
+        stage = [
+            [
+                after(row[i + 1], row[i]) if i + 1 < len(row) else row[i]
+                for i in range(0, len(row), 2)
+            ]
+            for row in stage
+        ]
+        tree.append(stage)
+    whole = [row[0] for row in stage]
+
+    def reaching(p, i):
+        result, done = None, 0
+        for depth in range(len(tree) - 1, -1, -1):
+            if i - done >= 1 << depth:
+                piece = tree[depth][p][done >> depth]
+                result = piece if result is None else after(piece, result)
+                done += 1 << depth
+        return result
+
     compact = [m[:HEAD_CHANNELS] + m[HEAD_CHANNELS:] for m in whole]
 
     def finish():
@@ -656,8 +702,9 @@
             removed = pair_dot(out_bs[n], parts)
             carry = r_outs[n] - removed[:, :wide]
             value = out_vs[n] - removed[:, wide:]
-            if heads_at[n] is not None:
-                moved = pair_dot(carry, split_parts(heads_at[n]))
+            entry = reaching(items[n][1], items[n][0])
+            if entry is not None:
+                moved = pair_dot(carry, split_parts(entry))
                 carry = moved[:, :wide]
                 value = value + moved[:, wide:]
             results[items[n]] = (carry, value)
@@ -742,7 +789,7 @@
         pltpu.make_async_copy(source, target, load_sem.at[n])
         for n, (source, target) in enumerate(zip(inputs, copies))
     ]
-    for n in (11, 12, 13, 14, 0, 1, 2, 3, 4, 6, 7, 18, 19, 20, 15, 16, 17, 5, 8, 9, 10):
+    for n in (13, 14, 11, 12, 0, 1, 2, 3, 4, 6, 7, 18, 19, 20, 15, 16, 17, 5, 8, 9, 10):
         loads[n].start()
 
     def rows_of(bits):
@@ -778,9 +825,8 @@
             {"tp": partner},
         )
 
-    for n in (11, 12, 13, 14):
+    for n in (13, 14):
         loads[n].wait()
-    normed[...] = rms_scale(x_ref[...], egain_ref[...]).astype(jnp.bfloat16)
     chosen_count = idx_ref.shape[0]
     experts = 2 * ep_count
     expert_row = lax.broadcasted_iota(jnp.int32, (experts, tok_rows), 0)
@@ -805,6 +851,9 @@
         lax.broadcasted_iota(jnp.int32, (slots, tok_rows), 0) % capacity
     ).astype(jnp.float32)
     placing = jnp.where(mm(mine, rank) == slot_rank, 1.0, 0.0).astype(jnp.bfloat16)
+    for n in (11, 12):
+        loads[n].wait()
+    normed[...] = rms_scale(x_ref[...], egain_ref[...]).astype(jnp.bfloat16)
     fold_span = pl.ds(pl.multiple_of(half * fold, fold), fold)
     other_span = pl.ds(pl.multiple_of(other * fold, fold), fold)
     outgoing[...] = mm(placing, normed[:, fold_span]).astype(jnp.bfloat16)
@@ -888,6 +937,16 @@
                 dispatch(bits).wait_recv()
                 forward(bits).start()
 
+    for turn in (1, 0):
+        shared_cross(turn).wait_recv()
+        shared_sum[turn] = shared[tp_of(turn)].astype(jnp.float32) + shared_half[turn].astype(
+            jnp.float32
+        )
+    shared_last[0] = shared_sum[1].astype(jnp.bfloat16)
+    shared_tail = remote(
+        shared_last.at[0], shared_last.at[1], tail_send.at[0], tail_recv.at[0], {"tp": across}
+    )
+    shared_tail.start()
     take_in(first_batch)
 
     @pl.when(outer == 1)
@@ -960,16 +1019,6 @@
         loads[n].wait()
     wait_far(first_batch)
     feed(0, first_batch)
-    for turn in (1, 0):
-        shared_cross(turn).wait_recv()
-        shared_sum[turn] = shared[tp_of(turn)].astype(jnp.float32) + shared_half[turn].astype(
-            jnp.float32
-        )
-    shared_last[0] = shared_sum[1].astype(jnp.bfloat16)
-    shared_tail = remote(
-        shared_last.at[0], shared_last.at[1], tail_send.at[0], tail_recv.at[0], {"tp": across}
-    )
-    shared_tail.start()
     def moved_by(block, p, current):
         through = block[p, :, :wide]
         high, low = pair_parts(current, masks)
@@ -1076,11 +1125,11 @@
         attend()
 
     take_in(near_batch)
-    wait_far(near_batch)
     @pl.when(level == 0)
     def _():
         pass_mix()
 
+    wait_far(near_batch)
     feed(1, near_batch)
     take_in(second_batch)
     send_home(1, near_batch)
@@ -1224,8 +1273,8 @@
     return pl.pallas_call(
         functools.partial(mega_kernel, ep_count),
         out_shape=(
-            jax.ShapeDtypeStruct((rows // 4, model_width), bf16),
-            jax.ShapeDtypeStruct((tok_rows, columns), bf16),
+            pltpu.VMEM((rows // 4, model_width), bf16),
+            pltpu.VMEM((tok_rows, columns), bf16),
         ),
         in_specs=[pl.BlockSpec(memory_space=pl.ANY)] * len(operands),
         out_specs=(full, full),

time: 38.9 us -> 37 us (0.951)
  local copies, waits for them, and re-layouts: 2.36 us -> 1.36 us
  Pallas kernels: 35.6 us -> 34.8 us
    unnamed x4 -> x2, local copies, waits for them, and re-layouts: 2.36 us -> 1.36 us
    pallas_call x1, Pallas kernels: 35.6 us -> 34.8 us  [mega(): pl.pallas_call(functools.partial(mega_kernel, ep_count), out_shape=(pltpu...]
where the time goes in v3:
time: 37 us; the launch traced here: 36.8 us
  Pallas kernels  34.8 us (94%)
  local copies, waits for them, and re-layouts  1.36 us (4%)
  between operations  0.65 us (2%)
    pallas_call x1, Pallas kernels, mega(): pl.pallas_call(functools.partial(mega_kernel, ep_count), out_shape=(pltpu...  34.8 us
    unnamed x2, local copies, waits for them, and re-layouts  1.36 us

profile of v3, /device:TPU:17, one launch (start us, length us, event | category | flops | bytes accessed | tf_op | source)
XLA Modules:
  0.0 36.8 jit_solution(12534883154658178669)
XLA Ops:
  0.6 34.8 %shard_map.212 = (bf16[64,2048]{1,0:T(8,128)(2,1)S(1)}, bf16[128,512]{1,0:T(8,128)(2,1)S(1)}) custom-call(bf16[256,256]{1,0:T(8,128)(2,1)} %refs_0_.1, bf16[256,256]{1,0:T(8,128)(2,1)} %refs_1_.1, bf16[256,256]{1,0:T(8,128)(2,1)} %refs_2_.1, bf16[256,256]{1,0:T(8,128)(2,1)} %refs_3_.1, bf16[256,256]{1,0:T(8,128)(2,1)} %refs_4_.1, bf16[256,256]{1,0:T(8,128)(2,1)} %refs_5_.1, ...), custom_call_target="tpu_custom_call" | custom-call | tf_op jit(solution)/shard_map/pallas_call | solution.py:1273
  35.4 0.7 %copy.25 = bf16[64,2048]{1,0:T(8,128)(2,1)} copy(bf16[64,2048]{1,0:T(8,128)(2,1)S(1)} %get-tuple-element.2) | data formatting | bytes 524288
  36.1 0.7 %copy.26 = bf16[128,512]{1,0:T(8,128)(2,1)} copy(bf16[128,512]{1,0:T(8,128)(2,1)S(1)} %get-tuple-element.3) | data formatting | bytes 262144

commit v4 on v3

--- a/solution.py
+++ b/solution.py
@@ -1066,7 +1066,6 @@
         base_state[...] = jnp.zeros_like(base_state)
         settle()
 
-    send_home(0, first_batch)
     for n in (5, 8, 9, 10):
         loads[n].wait()
 
@@ -1124,6 +1123,7 @@
     def _():
         attend()
 
+    send_home(0, first_batch)
     take_in(near_batch)
     @pl.when(level == 0)
     def _():
@@ -1134,6 +1134,17 @@
     take_in(second_batch)
     send_home(1, near_batch)
 
+    last_first = (level > 0) & (outer == 1)
+
+    def feed_last():
+        wait_far(second_batch)
+        feed(2, second_batch)
+        send_home(2, second_batch)
+
+    @pl.when(last_first)
+    def _():
+        feed_last()
+
     @pl.when(level > 0)
     def _():
         above(0).wait_recv()
@@ -1143,13 +1154,14 @@
     def _():
         attend()
 
-    wait_far(second_batch)
-    feed(2, second_batch)
     @pl.when(level > 0)
     def _():
         pass_mix()
 
-    send_home(2, second_batch)
+    @pl.when(jnp.logical_not(last_first))
+    def _():
+        feed_last()
+
     mix_cross(0).wait_recv()
     mix_sum[...] = mix[place].astype(jnp.float32) + mix_half[0].astype(jnp.float32)
 
@@ -1169,11 +1181,16 @@
     ]
     shared_tail.wait_recv()
     base = shared_sum[0] + shared_last[1].astype(jnp.float32)
-    for batch in (first_batch, near_batch, second_batch):
-        for turn in range(2):
-            for bits in batch:
-                if not isinstance(bits, int) or bits or turn:
-                    home(turn, bits).wait_recv()
+    for turn in range(2):
+        for bits in first_batch:
+            home(turn, bits).wait_recv()
+    for turn in range(2):
+        for bits in near_batch:
+            if bits or turn:
+                home(turn, bits).wait_recv()
+    for turn in range(2):
+        for bits in second_batch:
+            home(turn, bits).wait_recv()
     returned = back[...].reshape(all_slots, columns)
     routed = mm(
         jnp.concatenate(picks, axis=1), jnp.concatenate([returned, returned], axis=0)

time: 37 us -> 36.6 us (0.989)
  Pallas kernels: 34.8 us -> 34.4 us
where the time goes in v4:
time: 36.6 us; the launch traced here: 36.5 us
  Pallas kernels  34.4 us (94%)
  local copies, waits for them, and re-layouts  1.36 us (4%)
  between operations  0.65 us (2%)
    pallas_call x1, Pallas kernels, mega(): pl.pallas_call(functools.partial(mega_kernel, ep_count), out_shape=(pltpu...  34.4 us
    unnamed x2, local copies, waits for them, and re-layouts  1.36 us

profile of v4, /device:TPU:17, one launch (start us, length us, event | category | flops | bytes accessed | tf_op | source)
XLA Modules:
  0.0 36.5 jit_solution(4744144568150891551)
XLA Ops:
  0.6 34.4 %shard_map.212 = (bf16[64,2048]{1,0:T(8,128)(2,1)S(1)}, bf16[128,512]{1,0:T(8,128)(2,1)S(1)}) custom-call(bf16[256,256]{1,0:T(8,128)(2,1)} %refs_0_.1, bf16[256,256]{1,0:T(8,128)(2,1)} %refs_1_.1, bf16[256,256]{1,0:T(8,128)(2,1)} %refs_2_.1, bf16[256,256]{1,0:T(8,128)(2,1)} %refs_3_.1, bf16[256,256]{1,0:T(8,128)(2,1)} %refs_4_.1, bf16[256,256]{1,0:T(8,128)(2,1)} %refs_5_.1, ...), custom_call_target="tpu_custom_call" | custom-call | tf_op jit(solution)/shard_map/pallas_call | solution.py:1290
  35.1 0.7 %copy.25 = bf16[64,2048]{1,0:T(8,128)(2,1)} copy(bf16[64,2048]{1,0:T(8,128)(2,1)S(1)} %get-tuple-element.2) | data formatting | bytes 524288
  35.8 0.7 %copy.26 = bf16[128,512]{1,0:T(8,128)(2,1)} copy(bf16[128,512]{1,0:T(8,128)(2,1)S(1)} %get-tuple-element.3) | data formatting | bytes 262144

commit v5 on v4

--- a/solution.py
+++ b/solution.py
@@ -734,7 +734,7 @@
     (
         normed, outgoing, arrived, carry_ref, value_ref, own_map, held, base_state, state,
         next_state, shared, shared_half, shared_sum, shared_last, crossing,
-        halves, own_ref, final, back, heads_ref, mix, mix_half, mix_sum, mix_last,
+        halves, own_ref, final, back, heads_ref, scale_ref, mix, mix_half, mix_sum, mix_last,
         load_sem, disp_send, disp_recv, fwd_send, fwd_recv, map_send, map_recv, base_send,
         base_recv, sh_send, sh_recv, cross_send, cross_recv, home_send, home_recv, mx_send,
         mx_recv, tail_send, tail_recv,
@@ -947,6 +947,9 @@
         shared_last.at[0], shared_last.at[1], tail_send.at[0], tail_recv.at[0], {"tp": across}
     )
     shared_tail.start()
+    for n in (5, 8):
+        loads[n].wait()
+    scale_ref[...] = hgain_ref[...] * jax.nn.sigmoid(gate_ref[...].astype(jnp.float32))
     take_in(first_batch)
 
     @pl.when(outer == 1)
@@ -1066,7 +1069,7 @@
         base_state[...] = jnp.zeros_like(base_state)
         settle()
 
-    for n in (5, 8, 9, 10):
+    for n in (9, 10):
         loads[n].wait()
 
     def mix_cross(turn):
@@ -1101,8 +1104,7 @@
             heads_ref[:, lanes] = (
                 centred
                 * lax.rsqrt(spread + GROUP_EPSILON)
-                * hgain_ref[:, lanes]
-                * jax.nn.sigmoid(gate_ref[:, lanes].astype(jnp.float32))
+                * scale_ref[:, lanes]
             ).astype(jnp.bfloat16)
         for turn in (1, 0):
             project(turn)
@@ -1274,6 +1276,7 @@
         pltpu.VMEM((2, slots, columns), bf16),
         pltpu.VMEM((2, slots, columns), bf16),
         pltpu.VMEM((rows, width), bf16),
+        pltpu.VMEM((rows, width), f32),
         pltpu.VMEM((4, rows // 4, model_width), bf16),
         pltpu.VMEM((2, rows // 4, model_width), bf16),
         pltpu.VMEM((rows // 4, model_width), f32),

time: 36.6 us -> 36.6 us (level)
  no operation moved by 1% of the time
where the time goes in v5:
time: 36.6 us; the launch traced here: 36.4 us
  Pallas kernels  34.4 us (94%)
  local copies, waits for them, and re-layouts  1.36 us (4%)
  between operations  0.65 us (2%)
    pallas_call x1, Pallas kernels, mega(): pl.pallas_call(functools.partial(mega_kernel, ep_count), out_shape=(pltpu...  34.4 us
    unnamed x2, local copies, waits for them, and re-layouts  1.36 us

profile of v5, /device:TPU:17, one launch (start us, length us, event | category | flops | bytes accessed | tf_op | source)
XLA Modules:
  0.0 36.4 jit_solution(3445456017035638389)
XLA Ops:
  0.6 34.4 %shard_map.212 = (bf16[64,2048]{1,0:T(8,128)(2,1)S(1)}, bf16[128,512]{1,0:T(8,128)(2,1)S(1)}) custom-call(bf16[256,256]{1,0:T(8,128)(2,1)} %refs_0_.1, bf16[256,256]{1,0:T(8,128)(2,1)} %refs_1_.1, bf16[256,256]{1,0:T(8,128)(2,1)} %refs_2_.1, bf16[256,256]{1,0:T(8,128)(2,1)} %refs_3_.1, bf16[256,256]{1,0:T(8,128)(2,1)} %refs_4_.1, bf16[256,256]{1,0:T(8,128)(2,1)} %refs_5_.1, ...), custom_call_target="tpu_custom_call" | custom-call | tf_op jit(solution)/shard_map/pallas_call | solution.py:1293
  35.1 0.7 %copy.25 = bf16[64,2048]{1,0:T(8,128)(2,1)} copy(bf16[64,2048]{1,0:T(8,128)(2,1)S(1)} %get-tuple-element.2) | data formatting | bytes 524288
  35.8 0.7 %copy.26 = bf16[128,512]{1,0:T(8,128)(2,1)} copy(bf16[128,512]{1,0:T(8,128)(2,1)S(1)} %get-tuple-element.3) | data formatting | bytes 262144
